TPU v7x, 256 devices: a whole 4x4x8 slice. The times are simulated.
256 devices in a mesh: gr: 2 (over z_hi), sp: 16 (over z_lo, y), tp: 8 (over x, core).
Axes of the slice: x: 4, y: 4, z: 8 (z_hi: 2, z_lo: 4; z = z_hi * 4 + z_lo), core: 2. Of those that a mesh axis runs over, the one named last changes fastest.
Arguments:
- context_input_tensor: bfloat16 [16, 16384, 2048], P(('gr', 'tp'), 'sp'), parts along dimension 0, may hold values from -8 to 8
- content_mapping_matrix: bfloat16 [2048, 1024], replicated, may hold values from -0.125 to 0.125
- address_mapping_matrix: bfloat16 [2048, 256], replicated, may hold values from -0.125 to 0.125
- increment_mapping_matrix: bfloat16 [2048, 16], replicated, may hold values from -0.125 to 0.125
- increment_speed_offset: float32 [16], P('sp'), may hold values from -1 to 0.5
- channel_fading_exponent: float32 [16], P('sp'), may hold values from -12 to -2
- extra_damping_spikes: float32 [16, 16, 16384], P(('gr', 'tp'), 'sp'), parts along dimension 0, may hold values from -3 to 0
- content_smoothing_coefficients: float32 [5, 16, 64], P(None, 'sp'), may hold values from -2.5 to 2.5
- address_smoothing_coefficients: float32 [5, 4, 64], replicated, may hold values from -2.5 to 2.5
- newest_lookup_matrix: bfloat16 [16, 4, 64], P(('gr', 'tp')), parts along dimension 0, may hold values from -6 to 6
- newest_output_switch: bfloat16 [16, 16, 64], P(('gr', 'tp'), 'sp'), parts along dimension 0, may hold values from -6 to 6
- cluster_scaling_coefficients: float32 [16, 64], P('sp'), may hold values from 0.1 to 1.9
Outputs:
- address_content_store: bfloat16 [16, 16384, 16, 128], P(('gr', 'tp'), None, 'sp'), parts along dimension 0
- earliest_switched_retrieval: bfloat16 [16, 16, 64], P(('gr', 'tp'), 'sp'), parts along dimension 0
There are 2 independent parts, one for each index of `gr`. A program takes and returns all parts, laid end to end along the dimension named above; an argument that names none is the same for every part. Nothing has to cross between parts.
All inputs are finite; a program needn't handle non-finite values.
Results may differ from a plain program's by a relative error of at most 0.009.
Values may be sent and summed in bfloat16 or wider, within the bound.
A program may use at most 128 MiB of HBM per device.

v0:
```python
import jax
import jax.numpy as jnp
from jax import lax
from jax.sharding import PartitionSpec as P

HEADS = 16
HEAD = 64
GROUPS = 4
STATE = 64


EPS = 1e-05


def swapped(value, axis, bit):
    mask = 2**bit
    pairs = [(source, source ^ mask) for source in range(lax.axis_size(axis))]
    return lax.ppermute(value, axis, pairs)


def centred(signal, kernel):
    margin = kernel.shape[0] // 2
    length = signal.shape[0]
    padded = jnp.pad(signal, ((margin, margin), (0, 0), (0, 0)))
    summed = kernel[0] * padded[0:length]
    for offset in range(1, kernel.shape[0]):
        summed = summed + kernel[offset] * padded[offset : offset + length]
    return summed


def on_device(
    context_input_tensor,
    content_mapping_matrix,
    address_mapping_matrix,
    increment_mapping_matrix,
    increment_speed_offset,
    channel_fading_exponent,
    extra_damping_spikes,
    content_smoothing_coefficients,
    address_smoothing_coefficients,
    newest_lookup_matrix,
    newest_output_switch,
    cluster_scaling_coefficients,
):
    prompt_token_rows = context_input_tensor[0]
    span_len = prompt_token_rows.shape[0]
    repeats = HEADS // GROUPS
    local_heads = increment_speed_offset.shape[0]
    group_devices = repeats // local_heads
    group_index = lax.axis_index("sp") * local_heads // repeats
    value_proj = (
        jnp.dot(prompt_token_rows, content_mapping_matrix, preferred_element_type=jnp.float32)
        .astype(jnp.bfloat16)
        .reshape(span_len, HEADS, HEAD)
    )
    key_proj = (
        jnp.dot(prompt_token_rows, address_mapping_matrix, preferred_element_type=jnp.float32)
        .astype(jnp.bfloat16)
        .reshape(span_len, GROUPS, STATE)
    )
    rate_raw = jnp.dot(
        prompt_token_rows, increment_mapping_matrix, preferred_element_type=jnp.float32
    ).astype(jnp.bfloat16)
    key_copies = jnp.repeat(key_proj, repeats, axis=1)
    value_seq, key_seq, rate_seq = (
        lax.all_to_all(value_proj, "sp", split_axis=1, concat_axis=0, tiled=True),
        lax.all_to_all(key_copies, "sp", split_axis=1, concat_axis=0, tiled=True),
        lax.all_to_all(rate_raw, "sp", split_axis=1, concat_axis=0, tiled=True),
    )
    kernel_key = lax.dynamic_slice_in_dim(address_smoothing_coefficients, group_index, 1, 1)
    value_conv = jax.nn.silu(
        centred(value_seq.astype(jnp.float32), content_smoothing_coefficients)
    ).astype(jnp.bfloat16)
    key_conv = jax.nn.silu(centred(key_seq.astype(jnp.float32), kernel_key)).astype(jnp.bfloat16)
    smoothed_increment_speed = jax.nn.softplus(
        rate_seq.astype(jnp.float32) + increment_speed_offset
    )
    exponent_increment_amount = (
        -jnp.exp(channel_fading_exponent) * smoothed_increment_speed + extra_damping_spikes[0].T
    )
    cumul = jnp.cumsum(exponent_increment_amount, axis=0)
    end_weight = jnp.exp(cumul[-1] - cumul)
    weighted = (
        value_conv.astype(jnp.float32) * (smoothed_increment_speed * end_weight)[:, :, None]
    ).astype(jnp.bfloat16)
    states = jnp.einsum("lhp,lhn->hpn", weighted, key_conv, preferred_element_type=jnp.float32)
    query_vector_row = lax.dynamic_slice_in_dim(newest_lookup_matrix[0], group_index, 1, 0).astype(
        jnp.float32
    )
    raw_read = jnp.einsum("hpn,hn->hp", states, query_vector_row, precision=lax.Precision.HIGHEST)
    gated_read = raw_read * jax.nn.silu(newest_output_switch[0].astype(jnp.float32))
    group_sq = jnp.sum(gated_read * gated_read).reshape(1)
    for level in range(group_devices.bit_length() - 1):
        group_sq = group_sq + swapped(group_sq, "sp", level)
    scaled = (
        gated_read * lax.rsqrt(group_sq[0] / (repeats * HEAD) + EPS) * cluster_scaling_coefficients
    )
    kv_rows = jnp.concatenate([value_conv, key_conv], axis=-1)
    return (kv_rows[None], scaled.astype(jnp.bfloat16)[None])


def solution(mesh):
    placed = (
        P(("gr", "tp"), "sp", None),
        P(),
        P(),
        P(),
        P("sp"),
        P("sp"),
        P(("gr", "tp"), "sp", None),
        P(None, "sp", None),
        P(),
        P(("gr", "tp"), None, None),
        P(("gr", "tp"), "sp", None),
        P("sp", None),
    )
    return jax.shard_map(
        on_device,
        mesh=mesh,
        in_specs=placed,
        out_specs=(P(("gr", "tp"), None, "sp", None), P(("gr", "tp"), "sp", None)),
        check_vma=False,
    )
```

profile of v0, /device:TPU:38, one launch (start us, length us, event | category | flops | bytes accessed | tf_op | source)
XLA Modules:
  0.0 170.7 jit_solution(4248293259169450705)
XLA Ops:
  0.6 0.0 copy-start
  0.6 3.5 %fusion.22 = bf16[1024,16,1]{0,1,2:T(8,128)(2,1)S(1)} fusion(bf16[2048,16]{0,1:T(8,128)(2,1)} %param.15, bf16[1,1024,2048]{2,1,0:T(8,128)(2,1)} %param.12), kind=kOutput, calls=%fused_computation.23 | convolution fusion | flops 67125248 | bytes 4292608 | tf_op jit(solution)/shard_map/dot_general | solution.py:61
  4.1 0.1 copy.57
  4.2 0.5 broadcast.123
  4.7 0.8 reduce.2
  5.5 0.6 reshape.372
  6.2 8.7 %all-to-all-start.2 = ((bf16[16,2,512]{2,1,0:T(2,128)(2,1)}), bf16[16,2,512]{2,1,0:T(2,128)(2,1)S(1)}, u32[]{:S(2)}, u32[]{:S(2)}) async-start(bf16[16,2,512]{2,1,0:T(2,128)(2,1)} %reshape.372), calls=%async_computation.2 | async-start | bytes 65536 | tf_op jit(solution)/shard_map/all_to_all | solution.py:68
  14.8 0.0 copy-done
  14.8 3.5 %fusion.16 = bf16[1024,256]{0,1:T(8,128)(2,1)S(1)} fusion(bf16[2048,256]{1,0:T(8,128)(2,1)S(1)} %copy-done, bf16[1,1024,2048]{2,1,0:T(8,128)(2,1)} %param.12), kind=kOutput, calls=%fused_computation.21 | convolution fusion | flops 1074003968 | bytes 5767168 | tf_op jit(solution)/shard_map/dot_general | solution.py:57
  18.3 3.1 %all-to-all-done.2 = bf16[16,2,512]{2,1,0:T(2,128)(2,1)S(1)} async-done(((bf16[16,2,512]{2,1,0:T(2,128)(2,1)}), bf16[16,2,512]{2,1,0:T(2,128)(2,1)S(1)}, u32[]{:S(2)}, u32[]{:S(2)}) %all-to-all-start.2) | async-done | bytes 32800 | tf_op jit(solution)/shard_map/all_to_all | solution.py:68
  21.4 1.6 broadcast_in_dim.12
  22.9 5.2 %all-to-all-start.1 = ((bf16[1024,16,64]{0,2,1:T(8,128)(2,1)}), bf16[1024,16,64]{0,2,1:T(8,128)(2,1)S(1)}, u32[]{:S(2)}, u32[]{:S(2)}) async-start(bf16[1024,16,64]{0,2,1:T(8,128)(2,1)} %bitcast.123), calls=%async_computation.1 | async-start | bytes 4194304 | tf_op jit(solution)/shard_map/all_to_all | solution.py:67
  28.2 9.3 %fusion.13 = bf16[1024,1024]{0,1:T(8,128)(2,1)} fusion(bf16[2048,1024]{1,0:T(8,128)(2,1)} %param.13, bf16[1,1024,2048]{2,1,0:T(8,128)(2,1)} %param.12), kind=kOutput, calls=%fused_computation.20 | convolution fusion | flops 4296015872 | bytes 10485760 | tf_op jit(solution)/shard_map/dot_general | solution.py:52
  37.5 0.0 copy-start.3
  37.5 0.0 copy-start.4
  37.5 36.8 %all-to-all-done.1 = bf16[1024,16,64]{0,2,1:T(8,128)(2,1)S(1)} async-done(((bf16[1024,16,64]{0,2,1:T(8,128)(2,1)}), bf16[1024,16,64]{0,2,1:T(8,128)(2,1)S(1)}, u32[]{:S(2)}, u32[]{:S(2)}) %all-to-all-start.1) | async-done | bytes 2097184 | tf_op jit(solution)/shard_map/all_to_all | solution.py:67
  74.3 6.1 %all-to-all-start = ((bf16[1024,16,64]{0,2,1:T(8,128)(2,1)}), bf16[1024,16,64]{0,2,1:T(8,128)(2,1)}, u32[]{:S(2)}, u32[]{:S(2)}) async-start(bf16[1024,16,64]{0,2,1:T(8,128)(2,1)} %bitcast.124), calls=%async_computation | async-start | bytes 4194304 | tf_op jit(solution)/shard_map/all_to_all | solution.py:66
  81.1 0.0 copy-done.3
  81.1 0.1 copy.50
  81.9 0.8 fusion.34
  82.6 0.0 copy-done.4
  82.7 0.1 convert_add_fusion
  82.8 0.1 copy.45
  82.9 0.1 fusion.28
  82.9 0.2 reduce-window.6
  83.1 0.1 copy.51
  83.2 0.3 reduce-window.9
  83.5 0.1 broadcast.121
  83.6 0.6 slice.90
  84.2 0.6 slice.89
  86.1 0.1 fusion.26
  86.2 0.5 convert_bitcast_fusion
  86.7 2.3 %copy.55 = f32[1,16,8,8,1024]{4,3,1,2,0:T(8,128)} copy(f32[1,16,8,8,1024]{4,3,2,1,0:T(8,128)S(1)} %convert_bitcast_fusion) | data formatting | bytes 8388608 | tf_op jit(solution)/shard_map/convert_element_type | solution.py:74
  89.0 37.9 %all-to-all-done = bf16[1024,16,64]{0,2,1:T(8,128)(2,1)} async-done(((bf16[1024,16,64]{0,2,1:T(8,128)(2,1)}), bf16[1024,16,64]{0,2,1:T(8,128)(2,1)}, u32[]{:S(2)}, u32[]{:S(2)}) %all-to-all-start) | async-done | bytes 2097184 | tf_op jit(solution)/shard_map/all_to_all | solution.py:66
  126.9 2.0 %convert_bitcast_fusion.1 = f32[1,16,8,8,1024]{4,3,2,1,0:T(8,128)S(1)} fusion(bf16[1024,16,64]{0,2,1:T(8,128)(2,1)} %all-to-all-done), kind=kLoop, calls=%fused_computation.2 | loop fusion | flops 1048576 | bytes 6291456
  128.9 0.0 copy-start.1
  128.9 2.4 %copy.54 = f32[1,16,8,8,1024]{4,3,1,2,0:T(8,128)} copy(f32[1,16,8,8,1024]{4,3,2,1,0:T(8,128)S(1)} %convert_bitcast_fusion.1) | data formatting | bytes 8388608 | tf_op jit(solution)/shard_map/convert_element_type | solution.py:72
  131.4 1.3 copy-done.1
  132.6 18.0 %multiply_convert_fusion.1 = (bf16[16384,1,64]{0,2,1:T(8,128)(2,1)S(1)}, bf16[16384,1,64]{0,2,1:T(8,128)(2,1)}) fusion(f32[16384,1,64]{0,2,1:T(8,128)S(1)} %bitcast.121, f32[64]{0:T(128)S(1)} %get-tuple-element.8, f32[64]{0:T(128)S(1)} %get-tuple-element.5, f32[64]{0:T(128)S(1)} %get-tuple-element.6, f32[64]{0:T(128)S(1)} %get-tuple-element.7, ...), kind=kLoop, calls=%fused_computation.10 | loop fusion | flops 29360128 | bytes 12585472 | tf_op jit(solution)/shard_map/convert_element_type | solution.py:74
  150.6 0.0 copy-start.2
  150.6 3.9 %maximum_bitcast_fusion = bf16[1,16384,1,128]{1,3,2,0:T(8,128)(2,1)} fusion(bf16[16384,1,64]{0,2,1:T(8,128)(2,1)S(1)} %get-tuple-element.16, bf16[16384,1,64]{0,2,1:T(8,128)(2,1)} %get-tuple-element.17), kind=kLoop, calls=%fused_computation | loop fusion | flops 8388608 | bytes 8388608 | tf_op jit(solution)/shard_map/broadcast_in_dim | solution.py:99
  154.6 0.0 copy-done.2
  154.6 0.0 copy-start.5
  154.6 0.0 copy-start.7
  154.6 0.7 fusion.9
  155.3 0.0 copy-done.5
  155.3 0.0 copy-done.7
  155.3 0.8 multiply_reduce_fusion
  156.1 0.0 copy-start.6
  156.1 0.3 collective-permute-start
  156.3 6.4 %copy.53 = bf16[1,16384,1,128]{3,1,2,0:T(8,128)(2,1)} copy(bf16[1,16384,1,128]{1,3,2,0:T(8,128)(2,1)} %maximum_bitcast_fusion) | data formatting | bytes 8388608
  162.7 0.0 collective-permute-done
  164.0 5.3 %collective-permute-start.1 = (f32[1]{0:T(128)}, f32[1]{0:T(128)}, u32[]{:S(2)}, u32[]{:S(2)}) collective-permute-start(f32[1]{0:T(128)} %add.142), channel_id=1, source_target_pairs={{0,16},{8,24},{16,0},{24,8},{32,48},{40,56},{48,32},{56,40},{64,80... | collective-permute-start | bytes 20 | tf_op jit(solution)/shard_map/ppermute | solution.py:18
  169.2 0.2 collective-permute-done.1
  170.2 0.0 copy-done.6
  170.2 0.5 fusion.39
  (4 shorter events, 0.0 us)
Async XLA Ops:
  0.6 14.2 %copy-start = (bf16[2048,256]{1,0:T(8,128)(2,1)S(1)}, bf16[2048,256]{1,0:T(8,128)(2,1)}, u32[]{:S(2)}) copy-start(bf16[2048,256]{1,0:T(8,128)(2,1)} %param.14) | copy-start | bytes 3145732
  6.2 15.2 %all-to-all-start.2 = ((bf16[16,2,512]{2,1,0:T(2,128)(2,1)}), bf16[16,2,512]{2,1,0:T(2,128)(2,1)S(1)}, u32[]{:S(2)}, u32[]{:S(2)}) async-start(bf16[16,2,512]{2,1,0:T(2,128)(2,1)} %reshape.372), calls=%async_computation.2 | async-start | bytes 65536 | tf_op jit(solution)/shard_map/all_to_all | solution.py:68
  22.9 51.3 %all-to-all-start.1 = ((bf16[1024,16,64]{0,2,1:T(8,128)(2,1)}), bf16[1024,16,64]{0,2,1:T(8,128)(2,1)S(1)}, u32[]{:S(2)}, u32[]{:S(2)}) async-start(bf16[1024,16,64]{0,2,1:T(8,128)(2,1)} %bitcast.123), calls=%async_computation.1 | async-start | bytes 4194304 | tf_op jit(solution)/shard_map/all_to_all | solution.py:67
  37.5 43.6 %copy-start.3 = (f32[1,1,16384]{2,1,0:T(1,128)S(1)}, f32[1,1,16384]{2,1,0:T(1,128)}, u32[]{:S(2)}) copy-start(f32[1,1,16384]{2,1,0:T(1,128)} %param.18) | copy-start | bytes 196612
  37.5 45.1 %copy-start.4 = (f32[5,1,64]{2,1,0:T(1,128)S(1)}, f32[5,1,64]{2,1,0:T(1,128)}, u32[]{:S(2)}) copy-start(f32[5,1,64]{2,1,0:T(1,128)} %param.19) | copy-start | bytes 3844
  74.3 52.6 %all-to-all-start = ((bf16[1024,16,64]{0,2,1:T(8,128)(2,1)}), bf16[1024,16,64]{0,2,1:T(8,128)(2,1)}, u32[]{:S(2)}, u32[]{:S(2)}) async-start(bf16[1024,16,64]{0,2,1:T(8,128)(2,1)} %bitcast.124), calls=%async_computation | async-start | bytes 4194304 | tf_op jit(solution)/shard_map/all_to_all | solution.py:66
  128.9 3.7 %copy-start.1 = (f32[1,16,8,8,1024]{4,3,1,2,0:T(8,128)S(1)}, f32[1,16,8,8,1024]{4,3,1,2,0:T(8,128)}, u32[]{:S(2)}) copy-start(f32[1,16,8,8,1024]{4,3,1,2,0:T(8,128)} %copy.55) | copy-start | bytes 12582916
  150.6 3.9 %copy-start.2 = (bf16[16384,1,64]{0,2,1:T(8,128)(2,1)S(1)}, bf16[16384,1,64]{0,2,1:T(8,128)(2,1)}, u32[]{:S(2)}) copy-start(bf16[16384,1,64]{0,2,1:T(8,128)(2,1)} %get-tuple-element.17) | copy-start | bytes 6291460
  154.6 0.7 copy-start.5
  154.6 0.7 copy-start.7
  156.1 14.1 %copy-start.6 = (f32[1,64]{1,0:T(1,128)S(1)}, f32[1,64]{1,0:T(1,128)}, u32[]{:S(2)}) copy-start(f32[1,64]{1,0:T(1,128)} %param.23) | copy-start | bytes 772
  156.1 6.6 %collective-permute-start = (f32[1]{0:T(128)}, f32[1]{0:T(128)}, u32[]{:S(2)}, u32[]{:S(2)}) collective-permute-start(f32[1]{0:T(128)} %bitcast.42), channel_id=1, source_target_pairs={{0,8},{8,0},{16,24},{24,16},{32,40},{40,32},{48,56},{56,48},{64,72... | collective-permute-start | bytes 20 | tf_op jit(solution)/shard_map/ppermute | solution.py:18
  164.0 5.5 %collective-permute-start.1 = (f32[1]{0:T(128)}, f32[1]{0:T(128)}, u32[]{:S(2)}, u32[]{:S(2)}) collective-permute-start(f32[1]{0:T(128)} %add.142), channel_id=1, source_target_pairs={{0,16},{8,24},{16,0},{24,8},{32,48},{40,56},{48,32},{56,40},{64,80... | collective-permute-start | bytes 20 | tf_op jit(solution)/shard_map/ppermute | solution.py:18
where the time goes:
time: 172 us; the launch traced here: 171 us
  waiting for transfers between devices  77.9 us (45%)
  other arithmetic  26.5 us (15%)
  starting transfers between devices  25.5 us (15%)
  matrix products  17.7 us (10%)
  local copies, waits for them, and re-layouts  17.5 us (10%)
  between operations  5.47 us (3%)
    all_to_all x1, waiting for transfers between devices, on_device(): lax.all_to_all(value_proj, 'sp', split_axis=1, concat_axis=0, tiled=True)  37.9 us
    all_to_all x1, waiting for transfers between devices, on_device(): lax.all_to_all(key_copies, 'sp', split_axis=1, concat_axis=0, tiled=True)  36.8 us
    convert_element_type x1, other arithmetic, on_device(): jax.nn.silu(centred(key_seq.astype(jnp.float32), kernel_key))  18 us
    dot_general x1, matrix products, on_device(): jnp.dot(prompt_token_rows, content_mapping_matrix, preferred_element_type...  9.33 us
    unnamed x20, local copies, waits for them, and re-layouts  8.82 us
    all_to_all x1, starting transfers between devices, on_device(): lax.all_to_all(rate_raw, 'sp', split_axis=1, concat_axis=0, tiled=True)  8.65 us
    all_to_all x1, starting transfers between devices, on_device(): lax.all_to_all(value_proj, 'sp', split_axis=1, concat_axis=0, tiled=True)  6.12 us
    ppermute x2, starting transfers between devices, swapped(): return lax.ppermute(value, axis, pairs)  5.51 us
  transfers between devices with their start and end apart: 5, of which 4 were waited for; matrix products, arithmetic and copies ran while one was open for 15% of the time, Pallas kernels for 0%

commit v1 on v0

v1 whole, which is shorter than its diff:
```python
import functools

import jax
import jax.numpy as jnp
from jax import lax
from jax.experimental import pallas as pl
from jax.experimental.pallas import tpu as pltpu
from jax.sharding import PartitionSpec as P

HEADS = 16
HEAD = 64
GROUPS = 4
STATE = 64
KERNEL = 5
MODEL = 2048
SPAN = 1024
HALF = SPAN // 2
N = 16
Z = 4
Y = 4
LANES = 128
EPS = 1e-05
MESH = pl.DeviceIdType.MESH
CHUNK = 64


def mirror(place, side):
    return place + side * (3 - 2 * place)


def silu(v):
    return v / (1.0 + jnp.exp(-v))


def kernel(
    x_hbm,
    wv_hbm,
    wk_hbm,
    wr_hbm,
    offset_ref,
    fading_ref,
    spikes_hbm,
    vtaps_hbm,
    ktaps_hbm,
    query_hbm,
    switch_hbm,
    gain_hbm,
    kv_out,
    read_out,
    xb,
    wb,
    wr,
    spikes,
    vtaps_s,
    ktaps_s,
    query_s,
    switch_s,
    gain_s,
    acc,
    sb,
    rv,
    rk,
    notes,
    msend,
    mrecv,
    rates,
    weights,
    extv,
    extk,
    tapv,
    tapk,
    vw,
    kc,
    ob,
    states,
    qmat,
    gsend,
    grecv,
    in_sem,
    small_sem,
    k_send,
    v_send,
    f_send,
    m_send,
    k_recv,
    v_recv,
    m_recv,
    g_send,
    g_recv,
    o_sem,
):
    me = lax.axis_index("sp")
    z = me // Y
    y = me % Y
    core = lax.axis_index("tp") % 2
    side = z // 2
    zr = mirror(z, side)

    first = 3 - 2 * (1 - core) * (1 - zr)
    second = (1 - zr) * (3 - 2 * core) + 2 * zr
    third = 2 * (1 - zr)
    steps = [mirror(first, side), mirror(second, side), mirror(third, side), z]

    barrier = pltpu.get_barrier_semaphore()
    for i in range(1, N):
        pl.semaphore_signal(
            barrier, inc=1, device_id={"sp": (me + i) % N}, device_id_type=MESH
        )

    loads = []
    for i in range(4):
        rows = pl.ds(i * 256, 256)
        loads.append(pltpu.make_async_copy(x_hbm.at[rows], xb.at[rows], in_sem.at[i]))
    loads.append(pltpu.make_async_copy(wk_hbm, wb.at[0], in_sem.at[4]))
    for i in range(4):
        cols = pl.ds(pl.multiple_of(steps[i] * 256, 256), 256)
        loads.append(
            pltpu.make_async_copy(wv_hbm.at[:, cols], wb.at[i + 1], in_sem.at[5 + i])
        )
    for c in loads:
        c.start()
    smalls = [
        pltpu.make_async_copy(a, b, small_sem.at[i])
        for i, (a, b) in enumerate(
            [
                (wr_hbm, wr),
                (spikes_hbm, spikes),
                (vtaps_hbm, vtaps_s),
                (ktaps_hbm, ktaps_s),
                (query_hbm, query_s),
                (switch_hbm, switch_s),
                (gain_hbm, gain_s),
            ]
        )
    ]
    for c in smalls:
        c.start()

    def lo_mask(rows):
        return lax.broadcasted_iota(jnp.int32, (rows, LANES), 1) < HEAD

    def swap(v):
        return pltpu.roll(v, HEAD, 1)

    def remote(src, dst, ssem, rsem, peer):
        return pltpu.make_async_remote_copy(
            src_ref=src,
            dst_ref=dst,
            send_sem=ssem,
            recv_sem=rsem,
            device_id={"sp": peer},
            device_id_type=MESH,
        )

    def key_copy(zd):
        return remote(sb.at[zd], rk.at[me], k_send.at[zd], k_recv.at[me], zd * Y + y)

    def value_copy(slot, dest):
        return remote(sb.at[slot], rv.at[me], v_send.at[dest], v_recv.at[me], dest)

    def forward_copy(zs, j):
        s = zs * Y + y
        return remote(
            rk.at[s], rk.at[s], f_send.at[zs * Y + j], k_recv.at[s], z * Y + (y + j) % Y
        )

    def note_copy(dest):
        return remote(msend.at[dest], mrecv.at[me + 1], m_send.at[dest], m_recv.at[me], dest)

    notes[...] = jnp.zeros_like(notes)
    mrecv[0] = jnp.zeros((16, LANES), jnp.bfloat16)
    mrecv[N + 1] = jnp.zeros((16, LANES), jnp.bfloat16)

    for i in range(5):
        loads[i].wait()

    def tile(i, carry):
        for k in range(4):
            @pl.when(i == k + 1)
            def _():
                loads[5 + k].wait()

        acc[...] = jnp.dot(xb[...], wb[i], preferred_element_type=jnp.float32)
        low = lo_mask(CHUNK)

        def pack(c, carry2):
            r0 = pl.multiple_of(c * CHUNK, CHUNK)
            for pair in range(2):
                cols = slice(pair * LANES, (pair + 1) * LANES)
                top = acc[pl.ds(r0, CHUNK), cols]
                bot = acc[pl.ds(r0 + HALF, CHUNK), cols]
                even = jnp.where(low, top, swap(bot))
                odd = jnp.where(low, swap(top), bot)
                sb[4 * i + 2 * pair, pl.ds(r0, CHUNK)] = even.astype(jnp.bfloat16)
                sb[4 * i + 2 * pair + 1, pl.ds(r0, CHUNK)] = odd.astype(jnp.bfloat16)
            return carry2

        lax.fori_loop(0, HALF // CHUNK, pack, 0)

        low8 = lo_mask(8)
        edges = []
        for pair in range(2):
            cols = slice(pair * LANES, (pair + 1) * LANES)
            top = acc[0:8, cols]
            bot = pltpu.roll(acc[SPAN - 8 : SPAN, cols], 2, 0)
            edges.append(jnp.where(low8, bot, swap(top)))
            edges.append(jnp.where(low8, swap(bot), top))

        @pl.when(i == 0)
        def _():
            for g in range(GROUPS):
                for j in range(Y):
                    notes[g * Y + j, 10:12] = edges[g][0:2]
            pl.semaphore_wait(barrier, N - 1)
            for k in range(3):
                key_copy(steps[k]).start()

        zd = steps[0] * (i == 1) + steps[1] * (i == 2) + steps[2] * (i == 3) + z * (i == 4)

        @pl.when(i > 0)
        def _():
            for j in range(Y):
                notes[zd * Y + j, 8:10] = edges[j][0:2]

        @pl.when(jnp.logical_and(i > 0, i < 4))
        def _():
            for j in (2, 1, 3, 0):
                yd = (y + j) % Y
                value_copy(4 * i + yd, zd * Y + yd).start()

        @pl.when(i == 4)
        def _():
            for j in (2, 1, 3):
                yd = (y + j) % Y
                value_copy(16 + yd, z * Y + yd).start()

        @pl.when(i == 0)
        def _():
            rk[me] = sb[z]
            for j in (2, 1, 3):
                forward_copy(z, j).start()

        return carry

    lax.fori_loop(0, 5, tile, 0)
    rv[me] = sb[16 + y]

    for c in smalls:
        c.wait()

    raw = lax.dot_general(
        wr[...], xb[...], (((1,), (1,)), ((), ())), preferred_element_type=jnp.float32
    )
    for b in range(8):
        block = raw[:, b * LANES : (b + 1) * LANES]
        for h in range(HEADS):
            notes[h, b : b + 1] = block[h : h + 1]
    msend[...] = notes[...].astype(jnp.bfloat16)
    for i in range(1, N):
        note_copy((me + i) % N).start()
    mrecv[me + 1] = msend[me]

    for i in range(3):
        near = [1 - zr, 2 + 0 * zr, 3 + 0 * zr][i]
        zs = mirror(near, side)
        s = zs * Y + y
        remote(sb.at[0], rk.at[s], k_send.at[0], k_recv.at[s], s).wait_recv()
        for j in (2, 1, 3):
            forward_copy(zs, j).start()

    for i in range(1, N):
        s = (me + i) % N
        remote(msend.at[0], mrecv.at[s + 1], m_send.at[0], m_recv.at[s], s).wait_recv()

    for s in range(N):
        rates[8 * s : 8 * s + 8] = mrecv[s + 1].astype(jnp.float32)[0:8]
    speed = rates[...] + offset_ref[0, 0]
    speed = jnp.maximum(speed, 0.0) + jnp.log1p(jnp.exp(-jnp.abs(speed)))
    log_step = -jnp.exp(jnp.full((1, LANES), fading_ref[0, 0], jnp.float32)) * speed + spikes[...]
    ri = lax.broadcasted_iota(jnp.int32, (LANES, LANES), 0)
    ci = lax.broadcasted_iota(jnp.int32, (LANES, LANES), 1)
    later_lane = (ri > ci).astype(jnp.float32)
    later_row = (ci > ri).astype(jnp.float32)
    inner = jnp.dot(
        log_step, later_lane, precision=lax.Precision.HIGHEST, preferred_element_type=jnp.float32
    )
    outer = jnp.dot(
        later_row, log_step, precision=lax.Precision.HIGHEST, preferred_element_type=jnp.float32
    )
    suffix = inner + jnp.sum(outer, axis=1, keepdims=True)
    weights[...] = speed * jnp.exp(suffix)

    for k in range(KERNEL):
        row = vtaps_s[k : k + 1, :]
        tapv[k : k + 1, :] = jnp.concatenate([row, row], axis=1)
        row = ktaps_s[k, pl.ds(z, 1), :]
        tapk[k : k + 1, :] = jnp.concatenate([row, row], axis=1)
    qrow = query_s[...].astype(jnp.float32)
    pick = lax.broadcasted_iota(jnp.int32, (GROUPS, STATE), 0) == z
    qrow = jnp.sum(jnp.where(pick, qrow, 0.0), axis=0, keepdims=True)
    qrow = jnp.concatenate([qrow, qrow], axis=1)
    qcol = jnp.transpose(jnp.broadcast_to(qrow, (LANES, LANES)))
    qmat[...] = jnp.where((ri < STATE) == (ci < HEAD), qcol, 0.0)
    states[...] = jnp.zeros_like(states)

    def out_copy(slot, s):
        rows = pl.ds(pl.multiple_of(s * SPAN, SPAN), SPAN)
        return pltpu.make_async_copy(ob.at[slot], kv_out.at[rows], o_sem.at[slot])

    def span_of(t):
        zi = t // Y
        ji = t % Y
        zz = z * (zi == 0) + mirror(1 - zr, side) * (zi == 1)
        zz = zz + mirror(3 - zr * 0, side) * (zi == 2) + mirror(2 + zr * 0, side) * (zi == 3)
        j = 0 * (ji == 0) + 1 * (ji == 1) + 3 * (ji == 2) + 2 * (ji == 3)
        return zz * Y + (y + j) % Y, j

    low_c = lo_mask(CHUNK)

    def process(t, carry):
        s, j = span_of(t)
        slot = t % 2

        @pl.when(j != 0)
        def _():
            remote(sb.at[0], rk.at[s], k_send.at[0], k_recv.at[s], s).wait_recv()

        @pl.when(t > 0)
        def _():
            remote(sb.at[0], rv.at[s], v_send.at[0], v_recv.at[s], s).wait_recv()

        @pl.when(t >= 2)
        def _():
            out_copy(slot, s).wait()

        before = mrecv[s].astype(jnp.float32)
        after = mrecv[s + 2].astype(jnp.float32)
        low8 = lo_mask(8)
        for buf, ext, row in ((rv, extv, 8), (rk, extk, 10)):
            block = buf[s].astype(jnp.float32)
            ext[8 : 8 + HALF] = block
            head = swap(block[0:8])
            tail = swap(block[HALF - 8 : HALF])
            edge_b = before[8:16]
            edge_a = after[8:16]
            if row == 8:
                edge_b = pltpu.roll(edge_b, 6, 0)
            else:
                edge_b = pltpu.roll(edge_b, 4, 0)
                edge_a = pltpu.roll(edge_a, 6, 0)
            ext[0:8] = jnp.where(low8, edge_b, tail)
            ext[8 + HALF : 16 + HALF] = jnp.where(low8, head, edge_a)

        w8 = weights[pl.ds(pl.multiple_of(8 * s, 8), 8)]
        wcols = jnp.transpose(jnp.concatenate([w8] * 16, axis=0))
        tv = [tapv[k : k + 1, :] for k in range(KERNEL)]
        tk = [tapk[k : k + 1, :] for k in range(KERNEL)]
        for c in range(HALF // CHUNK):
            r0 = c * CHUNK
            v = tv[0] * extv[r0 + 6 : r0 + 6 + CHUNK]
            kk = tk[0] * extk[r0 + 6 : r0 + 6 + CHUNK]
            for k in range(1, KERNEL):
                v = v + tv[k] * extv[r0 + 6 + k : r0 + 6 + k + CHUNK]
                kk = kk + tk[k] * extk[r0 + 6 + k : r0 + 6 + k + CHUNK]
            v = silu(v)
            kk = silu(kk)
            b = r0 // LANES
            p0 = r0 % LANES
            wl = wcols[p0 : p0 + CHUNK, b : b + 1]
            wh = wcols[p0 : p0 + CHUNK, b + 4 : b + 5]
            w = jnp.where(low_c, wl, wh)
            vb = v.astype(jnp.bfloat16)
            vw[r0 : r0 + CHUNK] = (vb.astype(jnp.float32) * w).astype(jnp.bfloat16)
            kc[r0 : r0 + CHUNK] = kk.astype(jnp.bfloat16)
            ob[slot, r0 : r0 + CHUNK] = jnp.where(low_c, v, swap(kk)).astype(jnp.bfloat16)
            ob[slot, HALF + r0 : HALF + r0 + CHUNK] = jnp.where(low_c, swap(v), kk).astype(
                jnp.bfloat16
            )
        out_copy(slot, s).start()
        states[...] += lax.dot_general(
            kc[...], vw[...], (((0,), (0,)), ((), ())), preferred_element_type=jnp.float32
        )
        return carry

    lax.fori_loop(0, N, process, 0)

    read = jnp.sum(states[...] * qmat[...], axis=0, keepdims=True)
    read = read + swap(read)
    gate = switch_s[...].astype(jnp.float32)
    gate = jnp.concatenate([gate, gate], axis=1)
    gated = read * silu(gate)
    square = 0.5 * jnp.sum(gated * gated, axis=1, keepdims=True)
    gsend[...] = jnp.broadcast_to(square, (8, LANES))

    def square_copy(j):
        return remote(
            gsend, grecv.at[y], g_send.at[j], g_recv.at[y], z * Y + (y + j) % Y
        )

    for j in (2, 1, 3):
        square_copy(j).start()
    grecv[y] = gsend[...]
    for j in (1, 2, 3):
        yy = (y + j) % Y
        remote(gsend, grecv.at[yy], g_send.at[0], g_recv.at[yy], me).wait_recv()
    total = grecv[0] + grecv[1] + grecv[2] + grecv[3]
    gain = gain_s[...]
    gain = jnp.concatenate([gain, gain], axis=1)
    scaled = gated * lax.rsqrt(total[0:1] / (HEAD * HEADS // GROUPS) + EPS) * gain
    read_out[...] = scaled[:, :HEAD].astype(jnp.bfloat16)

    out_copy(0, 0).wait()
    out_copy(1, 0).wait()
    for j in (1, 2, 3):
        square_copy(j).wait_send()
        value_copy(16, z * Y + (y + j) % Y).wait_send()
    for k in range(3):
        key_copy(steps[k]).wait_send()
        for j in range(Y):
            value_copy(4, steps[k] * Y + j).wait_send()
    for i in range(1, N):
        note_copy((me + i) % N).wait_send()
    for zs in range(Z):
        for j in (1, 2, 3):
            forward_copy(zs, j).wait_send()


def on_device(
    context_input_tensor,
    content_mapping_matrix,
    address_mapping_matrix,
    increment_mapping_matrix,
    increment_speed_offset,
    channel_fading_exponent,
    extra_damping_spikes,
    content_smoothing_coefficients,
    address_smoothing_coefficients,
    newest_lookup_matrix,
    newest_output_switch,
    cluster_scaling_coefficients,
):
    bf16, f32 = jnp.bfloat16, jnp.float32
    anywhere = pl.BlockSpec(memory_space=pl.ANY)
    scalar = pl.BlockSpec(memory_space=pltpu.SMEM)
    dma = pltpu.SemaphoreType.DMA
    kv, read = pl.pallas_call(
        kernel,
        out_shape=(
            jax.ShapeDtypeStruct((N * SPAN, LANES), bf16),
            jax.ShapeDtypeStruct((1, HEAD), bf16),
        ),
        in_specs=[anywhere] * 4 + [scalar] * 2 + [anywhere] * 6,
        out_specs=(anywhere, pl.BlockSpec(memory_space=pltpu.VMEM)),
        scratch_shapes=[
            pltpu.VMEM((SPAN, MODEL), bf16),
            pltpu.VMEM((5, MODEL, 256), bf16),
            pltpu.VMEM((HEADS, MODEL), bf16),
            pltpu.VMEM((LANES, LANES), f32),
            pltpu.VMEM((KERNEL, HEAD), f32),
            pltpu.VMEM((KERNEL, GROUPS, STATE), f32),
            pltpu.VMEM((GROUPS, STATE), bf16),
            pltpu.VMEM((1, HEAD), bf16),
            pltpu.VMEM((1, HEAD), f32),
            pltpu.VMEM((SPAN, 256), f32),
            pltpu.VMEM((20, HALF, LANES), bf16),
            pltpu.VMEM((N, HALF, LANES), bf16),
            pltpu.VMEM((N, HALF, LANES), bf16),
            pltpu.VMEM((N, 16, LANES), f32),
            pltpu.VMEM((N, 16, LANES), bf16),
            pltpu.VMEM((N + 2, 16, LANES), bf16),
            pltpu.VMEM((LANES, LANES), f32),
            pltpu.VMEM((LANES, LANES), f32),
            pltpu.VMEM((HALF + 16, LANES), f32),
            pltpu.VMEM((HALF + 16, LANES), f32),
            pltpu.VMEM((8, LANES), f32),
            pltpu.VMEM((8, LANES), f32),
            pltpu.VMEM((HALF, LANES), bf16),
            pltpu.VMEM((HALF, LANES), bf16),
            pltpu.VMEM((2, SPAN, LANES), bf16),
            pltpu.VMEM((LANES, LANES), f32),
            pltpu.VMEM((LANES, LANES), f32),
            pltpu.VMEM((8, LANES), f32),
            pltpu.VMEM((Y, 8, LANES), f32),
            dma((9,)),
            dma((7,)),
            dma((Z,)),
            dma((N,)),
            dma((N,)),
            dma((N,)),
            dma((N,)),
            dma((N,)),
            dma((N,)),
            dma((Y,)),
            dma((Y,)),
            dma((2,)),
        ],
        compiler_params=pltpu.CompilerParams(
            collective_id=0, has_side_effects=True, vmem_limit_bytes=60 * 1024 * 1024
        ),
        name="mixer",
    )(
        context_input_tensor[0],
        content_mapping_matrix,
        address_mapping_matrix,
        increment_mapping_matrix.T,
        increment_speed_offset.reshape(1, 1),
        channel_fading_exponent.reshape(1, 1),
        extra_damping_spikes.reshape(LANES, LANES),
        content_smoothing_coefficients.reshape(KERNEL, HEAD),
        address_smoothing_coefficients,
        newest_lookup_matrix[0],
        newest_output_switch[0],
        cluster_scaling_coefficients,
    )
    return (kv.reshape(1, N * SPAN, 1, LANES), read[None])


def solution(mesh):
    placed = (
        P(("gr", "tp"), "sp", None),
        P(),
        P(),
        P(),
        P("sp"),
        P("sp"),
        P(("gr", "tp"), "sp", None),
        P(None, "sp", None),
        P(),
        P(("gr", "tp"), None, None),
        P(("gr", "tp"), "sp", None),
        P("sp", None),
    )
    return jax.shard_map(
        on_device,
        mesh=mesh,
        in_specs=placed,
        out_specs=(P(("gr", "tp"), None, "sp", None), P(("gr", "tp"), "sp", None)),
        check_vma=False,
    )
```

time: 172 us -> 91.9 us (0.53)
  Pallas kernels: 0 us -> 83.1 us
  waiting for transfers between devices: 77.9 us -> 0 us
  other arithmetic: 26.5 us -> 0 us
  starting transfers between devices: 25.5 us -> 0 us
  matrix products: 17.7 us -> 0 us
  local copies, waits for them, and re-layouts: 17.5 us -> 5.53 us
  between operations: 5.47 us -> 1.94 us
    pallas_call x0 -> x1, Pallas kernels: none -> 83.1 us  [on_device(): pl.pallas_call(kernel, out_shape=(jax.ShapeDtypeStruct((N * SPAN, LANES),...]
    all_to_all x3 -> x0, waiting for transfers between devices: 77.7 us -> none  [the longest x1 37.9 us: on_device(): lax.all_to_all(value_proj, 'sp', split_axis=1, concat_axis=0, tiled=True)]
    all_to_all x3 -> x0, starting transfers between devices: 20 us -> none  [the longest x1 8.65 us: on_device(): lax.all_to_all(rate_raw, 'sp', split_axis=1, concat_axis=0, tiled=True)]
    convert_element_type x1 -> x0, other arithmetic: 18 us -> none  [on_device(): jax.nn.silu(centred(key_seq.astype(jnp.float32), kernel_key))]
    dot_general x5 -> x0, matrix products: 17.7 us -> none  [the longest x1 9.33 us: on_device(): jnp.dot(prompt_token_rows, content_mapping_matrix, preferred_element_type...]
    ppermute x2 -> x0, starting transfers between devices: 5.51 us -> none  [swapped(): return lax.ppermute(value, axis, pairs)]
    convert_element_type x2 -> x0, local copies, waits for them, and re-layouts: 4.78 us -> none  [the longest x1 2.44 us: on_device(): value_seq.astype(jnp.float32)]
    broadcast_in_dim x2 -> x0, other arithmetic: 4.46 us -> none  [on_device(): return (kv_rows[None], scaled.astype(jnp.bfloat16)[None])]
  transfers between devices with their start and end apart: 5 -> 0, of which waited for: 4 -> 0; matrix products, arithmetic and copies ran while one was open for 15% -> 0% of each run, Pallas kernels for 0% -> 0%
where the time goes in v1:
time: 91.9 us; the launch traced here: 90.6 us
  Pallas kernels  83.1 us (90%)
  local copies, waits for them, and re-layouts  5.53 us (6%)
  between operations  1.94 us (2%)
    pallas_call x1, Pallas kernels, on_device(): pl.pallas_call(kernel, out_shape=(jax.ShapeDtypeStruct((N * SPAN, LANES),...  83.1 us
    unnamed x5, local copies, waits for them, and re-layouts  5.53 us

profile of v1, /device:TPU:38, one launch (start us, length us, event | category | flops | bytes accessed | tf_op | source)
XLA Modules:
  0.0 90.6 jit_solution(11212229789001996374)
XLA Ops:
  1.9 1.3 %copy.16 = f32[5,1,64]{2,0,1:T(8,128)} copy(f32[5,1,64]{2,1,0:T(1,128)} %param.19) | data formatting | bytes 2560
  3.2 83.1 %mixer.1 = (bf16[16384,128]{1,0:T(8,128)(2,1)}, bf16[1,64]{1,0:T(2,128)(2,1)}) custom-call(bf16[1024,2048]{1,0:T(8,128)(2,1)} %bitcast.14, bf16[2048,1024]{1,0:T(8,128)(2,1)} %wv_hbm.1, bf16[2048,256]{1,0:T(8,128)(2,1)} %wk_hbm.1, bf16[16,2048]{1,0:T(8,128)(2,1)} %bitcast.16, f32[1,1]{1,0:T(1,128)} %bitcast.12.offset_ref, f32[1,1]{1,0:T(1,128)} %bitcast.13.fading_ref, ...), custom_call_target="tpu_custom_call" | custom-call | tf_op jit(solution)/shard_map/mixer/pallas_call | solution.py:446
  86.4 0.0 copy-start
  86.4 3.7 %copy.21 = bf16[1,16384,1,128]{3,1,2,0:T(8,128)(2,1)} copy(bf16[1,16384,1,128]{3,1,2,0:T(8,128)(2,1)} %bitcast.15) | data formatting | bytes 8388608
  90.1 0.0 copy-done
  90.1 0.5 copy.22
Async XLA Ops:
  86.4 3.8 %copy-start = (bf16[1,64]{1,0:T(2,128)(2,1)S(1)}, bf16[1,64]{1,0:T(2,128)(2,1)}, u32[]{:S(2)}) copy-start(bf16[1,64]{1,0:T(2,128)(2,1)} %get-tuple-element.5) | copy-start | bytes 388

commit v2 on v1

--- a/solution.py
+++ b/solution.py
@@ -22,6 +22,7 @@
 EPS = 1e-05
 MESH = pl.DeviceIdType.MESH
 CHUNK = 64
+NOTE = 48
 
 
 def mirror(place, side):
@@ -61,8 +62,9 @@
     rv,
     rk,
     notes,
-    msend,
-    mrecv,
+    nsend,
+    edge_v,
+    edge_k,
     rates,
     weights,
     extv,
@@ -71,7 +73,6 @@
     tapk,
     vw,
     kc,
-    ob,
     states,
     qmat,
     gsend,
@@ -79,15 +80,14 @@
     in_sem,
     small_sem,
     k_send,
+    n_send,
     v_send,
     f_send,
-    m_send,
     k_recv,
+    n_recv,
     v_recv,
-    m_recv,
     g_send,
     g_recv,
-    o_sem,
 ):
     me = lax.axis_index("sp")
     z = me // Y
@@ -152,8 +152,18 @@
             device_id_type=MESH,
         )
 
+    keys = pl.ds(0, HALF)
+    extra = pl.ds(HALF, NOTE)
+
     def key_copy(zd):
-        return remote(sb.at[zd], rk.at[me], k_send.at[zd], k_recv.at[me], zd * Y + y)
+        return remote(
+            sb.at[zd], rk.at[me, keys], k_send.at[zd], k_recv.at[me], zd * Y + y
+        )
+
+    def note_copy(zd):
+        return remote(
+            nsend.at[zd], rk.at[me, extra], n_send.at[zd], n_recv.at[me], zd * Y + y
+        )
 
     def value_copy(slot, dest):
         return remote(sb.at[slot], rv.at[me], v_send.at[dest], v_recv.at[me], dest)
@@ -164,22 +174,7 @@
             rk.at[s], rk.at[s], f_send.at[zs * Y + j], k_recv.at[s], z * Y + (y + j) % Y
         )
 
-    def note_copy(dest):
-        return remote(msend.at[dest], mrecv.at[me + 1], m_send.at[dest], m_recv.at[me], dest)
-
-    notes[...] = jnp.zeros_like(notes)
-    mrecv[0] = jnp.zeros((16, LANES), jnp.bfloat16)
-    mrecv[N + 1] = jnp.zeros((16, LANES), jnp.bfloat16)
-
-    for i in range(5):
-        loads[i].wait()
-
-    def tile(i, carry):
-        for k in range(4):
-            @pl.when(i == k + 1)
-            def _():
-                loads[5 + k].wait()
-
+    def multiply(i):
         acc[...] = jnp.dot(xb[...], wb[i], preferred_element_type=jnp.float32)
         low = lo_mask(CHUNK)
 
@@ -197,86 +192,108 @@
 
         lax.fori_loop(0, HALF // CHUNK, pack, 0)
 
-        low8 = lo_mask(8)
-        edges = []
+    low8 = lo_mask(8)
+
+    def edge_rows(head, tail):
+        out = []
         for pair in range(2):
             cols = slice(pair * LANES, (pair + 1) * LANES)
-            top = acc[0:8, cols]
-            bot = pltpu.roll(acc[SPAN - 8 : SPAN, cols], 2, 0)
-            edges.append(jnp.where(low8, bot, swap(top)))
-            edges.append(jnp.where(low8, swap(bot), top))
-
-        @pl.when(i == 0)
-        def _():
-            for g in range(GROUPS):
-                for j in range(Y):
-                    notes[g * Y + j, 10:12] = edges[g][0:2]
-            pl.semaphore_wait(barrier, N - 1)
-            for k in range(3):
-                key_copy(steps[k]).start()
-
-        zd = steps[0] * (i == 1) + steps[1] * (i == 2) + steps[2] * (i == 3) + z * (i == 4)
-
-        @pl.when(i > 0)
-        def _():
-            for j in range(Y):
-                notes[zd * Y + j, 8:10] = edges[j][0:2]
-
-        @pl.when(jnp.logical_and(i > 0, i < 4))
-        def _():
-            for j in (2, 1, 3, 0):
-                yd = (y + j) % Y
-                value_copy(4 * i + yd, zd * Y + yd).start()
-
-        @pl.when(i == 4)
-        def _():
-            for j in (2, 1, 3):
-                yd = (y + j) % Y
-                value_copy(16 + yd, z * Y + yd).start()
-
-        @pl.when(i == 0)
-        def _():
-            rk[me] = sb[z]
-            for j in (2, 1, 3):
-                forward_copy(z, j).start()
-
-        return carry
-
-    lax.fori_loop(0, 5, tile, 0)
-    rv[me] = sb[16 + y]
-
-    for c in smalls:
+            top = head[:, cols]
+            bot = pltpu.roll(tail[:, cols], 2, 0)
+            out.append(jnp.where(low8, bot, swap(top))[0:2])
+            out.append(jnp.where(low8, swap(bot), top)[0:2])
+        return out
+
+    notes[...] = jnp.zeros_like(notes)
+
+    for i in range(5):
+        loads[i].wait()
+    multiply(0)
+    pl.semaphore_wait(barrier, N - 1)
+    for k in range(3):
+        key_copy(steps[k]).start()
+    rk[me, 0:HALF] = sb[z]
+
+    for g, e in enumerate(edge_rows(acc[0:8], acc[SPAN - 8 : SPAN])):
+        notes[g, 40:42] = e
+    for c in loads[5:] + smalls:
         c.wait()
-
+    xe = jnp.concatenate([xb[0:16], xb[SPAN - 16 : SPAN]], axis=0)
+    for i in range(1, 5):
+        e32 = jnp.dot(xe, wb[i], preferred_element_type=jnp.float32)
+        for j, e in enumerate(edge_rows(e32[0:8], e32[24:32])):
+            notes[steps[i - 1], 32 + 2 * j : 34 + 2 * j] = e
     raw = lax.dot_general(
         wr[...], xb[...], (((1,), (1,)), ((), ())), preferred_element_type=jnp.float32
     )
     for b in range(8):
         block = raw[:, b * LANES : (b + 1) * LANES]
         for h in range(HEADS):
-            notes[h, b : b + 1] = block[h : h + 1]
-    msend[...] = notes[...].astype(jnp.bfloat16)
-    for i in range(1, N):
-        note_copy((me + i) % N).start()
-    mrecv[me + 1] = msend[me]
-
-    for i in range(3):
-        near = [1 - zr, 2 + 0 * zr, 3 + 0 * zr][i]
+            row = 8 * (h % Y) + b
+            notes[h // Y, row : row + 1] = block[h : h + 1]
+    nsend[...] = notes[...].astype(jnp.bfloat16)
+    for k in range(3):
+        note_copy(steps[k]).start()
+    rk[me, HALF:] = nsend[z]
+    for j in (2, 1, 3):
+        forward_copy(z, j).start()
+
+    def tile(i, carry):
+        multiply(i)
+        zd = steps[0] * (i == 1) + steps[1] * (i == 2) + steps[2] * (i == 3) + z * (i == 4)
+
+        @pl.when(i < 4)
+        def _():
+            for j in (2, 1, 3, 0):
+                yd = (y + j) % Y
+                value_copy(4 * i + yd, zd * Y + yd).start()
+
+        @pl.when(i == 4)
+        def _():
+            for j in (2, 1, 3):
+                yd = (y + j) % Y
+                value_copy(16 + yd, z * Y + yd).start()
+
+        return carry
+
+    lax.fori_loop(1, 5, tile, 0)
+    rv[me] = sb[16 + y]
+
+    for near in (1 - zr, 2 + 0 * zr, 3 + 0 * zr):
         zs = mirror(near, side)
         s = zs * Y + y
-        remote(sb.at[0], rk.at[s], k_send.at[0], k_recv.at[s], s).wait_recv()
+        remote(sb.at[0], rk.at[s, keys], k_send.at[0], k_recv.at[s], s).wait_recv()
+        remote(nsend.at[0], rk.at[s, extra], n_send.at[0], n_recv.at[s], s).wait_recv()
         for j in (2, 1, 3):
             forward_copy(zs, j).start()
-
-    for i in range(1, N):
-        s = (me + i) % N
-        remote(msend.at[0], mrecv.at[s + 1], m_send.at[0], m_recv.at[s], s).wait_recv()
-
-    for s in range(N):
-        rates[8 * s : 8 * s + 8] = mrecv[s + 1].astype(jnp.float32)[0:8]
-    speed = rates[...] + offset_ref[0, 0]
+    for zz in range(Z):
+        for j in (1, 2, 3):
+            s = zz * Y + (y + j) % Y
+            remote(rk.at[0], rk.at[s], f_send.at[0], k_recv.at[s], s).wait_recv()
+
+    edge_v[0] = jnp.zeros((8, LANES), jnp.float32)
+    edge_k[0] = jnp.zeros((8, LANES), jnp.float32)
+    edge_v[N + 1] = jnp.zeros((8, LANES), jnp.float32)
+    edge_k[N + 1] = jnp.zeros((8, LANES), jnp.float32)
+    row8 = lax.broadcasted_iota(jnp.int32, (8, LANES), 0)
+
+    def unpack(s, carry):
+        got = rk[s, HALF:].astype(jnp.float32)
+        mine = got[0:8] * (y == 0) + got[8:16] * (y == 1)
+        mine = mine + got[16:24] * (y == 2) + got[24:32] * (y == 3)
+        rates[pl.ds(pl.multiple_of(8 * s, 8), 8)] = mine
+        ends = got[32:40]
+        e0 = jnp.sum(jnp.where(row8 == 2 * y, ends, 0.0), axis=0, keepdims=True)
+        e1 = jnp.sum(jnp.where(row8 == 2 * y + 1, ends, 0.0), axis=0, keepdims=True)
+        even = row8 % 2 == 0
+        edge_v[s + 1] = jnp.where(even, e0, e1)
+        edge_k[s + 1] = jnp.where(even, got[40:41], got[41:42])
+        return carry
+
+    lax.fori_loop(0, N, unpack, 0)
+    speed = rates[...] + offset_ref[0]
     speed = jnp.maximum(speed, 0.0) + jnp.log1p(jnp.exp(-jnp.abs(speed)))
-    log_step = -jnp.exp(jnp.full((1, LANES), fading_ref[0, 0], jnp.float32)) * speed + spikes[...]
+    log_step = -jnp.exp(jnp.full((1, LANES), fading_ref[0], jnp.float32)) * speed + spikes[...]
     ri = lax.broadcasted_iota(jnp.int32, (LANES, LANES), 0)
     ci = lax.broadcasted_iota(jnp.int32, (LANES, LANES), 1)
     later_lane = (ri > ci).astype(jnp.float32)
@@ -291,7 +308,7 @@
     weights[...] = speed * jnp.exp(suffix)
 
     for k in range(KERNEL):
-        row = vtaps_s[k : k + 1, :]
+        row = vtaps_s[k]
         tapv[k : k + 1, :] = jnp.concatenate([row, row], axis=1)
         row = ktaps_s[k, pl.ds(z, 1), :]
         tapk[k : k + 1, :] = jnp.concatenate([row, row], axis=1)
@@ -303,54 +320,32 @@
     qmat[...] = jnp.where((ri < STATE) == (ci < HEAD), qcol, 0.0)
     states[...] = jnp.zeros_like(states)
 
-    def out_copy(slot, s):
-        rows = pl.ds(pl.multiple_of(s * SPAN, SPAN), SPAN)
-        return pltpu.make_async_copy(ob.at[slot], kv_out.at[rows], o_sem.at[slot])
-
     def span_of(t):
         zi = t // Y
         ji = t % Y
         zz = z * (zi == 0) + mirror(1 - zr, side) * (zi == 1)
         zz = zz + mirror(3 - zr * 0, side) * (zi == 2) + mirror(2 + zr * 0, side) * (zi == 3)
         j = 0 * (ji == 0) + 1 * (ji == 1) + 3 * (ji == 2) + 2 * (ji == 3)
-        return zz * Y + (y + j) % Y, j
+        return zz * Y + (y + j) % Y
 
     low_c = lo_mask(CHUNK)
 
     def process(t, carry):
-        s, j = span_of(t)
-        slot = t % 2
-
-        @pl.when(j != 0)
-        def _():
-            remote(sb.at[0], rk.at[s], k_send.at[0], k_recv.at[s], s).wait_recv()
+        s = span_of(t)
 
         @pl.when(t > 0)
         def _():
             remote(sb.at[0], rv.at[s], v_send.at[0], v_recv.at[s], s).wait_recv()
 
-        @pl.when(t >= 2)
-        def _():
-            out_copy(slot, s).wait()
-
-        before = mrecv[s].astype(jnp.float32)
-        after = mrecv[s + 2].astype(jnp.float32)
-        low8 = lo_mask(8)
-        for buf, ext, row in ((rv, extv, 8), (rk, extk, 10)):
-            block = buf[s].astype(jnp.float32)
+        for buf, ext, edge in ((rv, extv, edge_v), (rk, extk, edge_k)):
+            block = buf[s, 0:HALF].astype(jnp.float32)
             ext[8 : 8 + HALF] = block
             head = swap(block[0:8])
             tail = swap(block[HALF - 8 : HALF])
-            edge_b = before[8:16]
-            edge_a = after[8:16]
-            if row == 8:
-                edge_b = pltpu.roll(edge_b, 6, 0)
-            else:
-                edge_b = pltpu.roll(edge_b, 4, 0)
-                edge_a = pltpu.roll(edge_a, 6, 0)
-            ext[0:8] = jnp.where(low8, edge_b, tail)
-            ext[8 + HALF : 16 + HALF] = jnp.where(low8, head, edge_a)
-
+            ext[0:8] = jnp.where(low8, edge[s], tail)
+            ext[8 + HALF : 16 + HALF] = jnp.where(low8, head, edge[s + 2])
+
+        base = pl.multiple_of(s * SPAN, SPAN)
         w8 = weights[pl.ds(pl.multiple_of(8 * s, 8), 8)]
         wcols = jnp.transpose(jnp.concatenate([w8] * 16, axis=0))
         tv = [tapv[k : k + 1, :] for k in range(KERNEL)]
@@ -372,11 +367,10 @@
             vb = v.astype(jnp.bfloat16)
             vw[r0 : r0 + CHUNK] = (vb.astype(jnp.float32) * w).astype(jnp.bfloat16)
             kc[r0 : r0 + CHUNK] = kk.astype(jnp.bfloat16)
-            ob[slot, r0 : r0 + CHUNK] = jnp.where(low_c, v, swap(kk)).astype(jnp.bfloat16)
-            ob[slot, HALF + r0 : HALF + r0 + CHUNK] = jnp.where(low_c, swap(v), kk).astype(
+            kv_out[pl.ds(base + r0, CHUNK)] = jnp.where(low_c, v, swap(kk)).astype(jnp.bfloat16)
+            kv_out[pl.ds(base + HALF + r0, CHUNK)] = jnp.where(low_c, swap(v), kk).astype(
                 jnp.bfloat16
             )
-        out_copy(slot, s).start()
         states[...] += lax.dot_general(
             kc[...], vw[...], (((0,), (0,)), ((), ())), preferred_element_type=jnp.float32
         )
@@ -409,20 +403,21 @@
     scaled = gated * lax.rsqrt(total[0:1] / (HEAD * HEADS // GROUPS) + EPS) * gain
     read_out[...] = scaled[:, :HEAD].astype(jnp.bfloat16)
 
-    out_copy(0, 0).wait()
-    out_copy(1, 0).wait()
     for j in (1, 2, 3):
         square_copy(j).wait_send()
         value_copy(16, z * Y + (y + j) % Y).wait_send()
     for k in range(3):
         key_copy(steps[k]).wait_send()
+        note_copy(steps[k]).wait_send()
         for j in range(Y):
             value_copy(4, steps[k] * Y + j).wait_send()
-    for i in range(1, N):
-        note_copy((me + i) % N).wait_send()
     for zs in range(Z):
         for j in (1, 2, 3):
             forward_copy(zs, j).wait_send()
+
+
+def in_hbm(a):
+    return pltpu.with_memory_space_constraint(a, pltpu.HBM)
 
 
 def on_device(
@@ -440,23 +435,22 @@
     cluster_scaling_coefficients,
 ):
     bf16, f32 = jnp.bfloat16, jnp.float32
-    anywhere = pl.BlockSpec(memory_space=pl.ANY)
-    scalar = pl.BlockSpec(memory_space=pltpu.SMEM)
+    anywhere = pl.BlockSpec(memory_space=pltpu.HBM)
     dma = pltpu.SemaphoreType.DMA
     kv, read = pl.pallas_call(
         kernel,
         out_shape=(
-            jax.ShapeDtypeStruct((N * SPAN, LANES), bf16),
+            pltpu.VMEM((N * SPAN, LANES), bf16),
             jax.ShapeDtypeStruct((1, HEAD), bf16),
         ),
-        in_specs=[anywhere] * 4 + [scalar] * 2 + [anywhere] * 6,
-        out_specs=(anywhere, pl.BlockSpec(memory_space=pltpu.VMEM)),
+        in_specs=[anywhere] * 4 + [pl.BlockSpec(memory_space=pltpu.SMEM)] * 2 + [anywhere] * 6,
+        out_specs=(pl.BlockSpec(memory_space=pltpu.VMEM),) * 2,
         scratch_shapes=[
             pltpu.VMEM((SPAN, MODEL), bf16),
             pltpu.VMEM((5, MODEL, 256), bf16),
             pltpu.VMEM((HEADS, MODEL), bf16),
             pltpu.VMEM((LANES, LANES), f32),
-            pltpu.VMEM((KERNEL, HEAD), f32),
+            pltpu.VMEM((KERNEL, 1, HEAD), f32),
             pltpu.VMEM((KERNEL, GROUPS, STATE), f32),
             pltpu.VMEM((GROUPS, STATE), bf16),
             pltpu.VMEM((1, HEAD), bf16),
@@ -464,10 +458,11 @@
             pltpu.VMEM((SPAN, 256), f32),
             pltpu.VMEM((20, HALF, LANES), bf16),
             pltpu.VMEM((N, HALF, LANES), bf16),
-            pltpu.VMEM((N, HALF, LANES), bf16),
-            pltpu.VMEM((N, 16, LANES), f32),
-            pltpu.VMEM((N, 16, LANES), bf16),
-            pltpu.VMEM((N + 2, 16, LANES), bf16),
+            pltpu.VMEM((N, HALF + NOTE, LANES), bf16),
+            pltpu.VMEM((Z, NOTE, LANES), f32),
+            pltpu.VMEM((Z, NOTE, LANES), bf16),
+            pltpu.VMEM((N + 2, 8, LANES), f32),
+            pltpu.VMEM((N + 2, 8, LANES), f32),
             pltpu.VMEM((LANES, LANES), f32),
             pltpu.VMEM((LANES, LANES), f32),
             pltpu.VMEM((HALF + 16, LANES), f32),
@@ -476,7 +471,6 @@
             pltpu.VMEM((8, LANES), f32),
             pltpu.VMEM((HALF, LANES), bf16),
             pltpu.VMEM((HALF, LANES), bf16),
-            pltpu.VMEM((2, SPAN, LANES), bf16),
             pltpu.VMEM((LANES, LANES), f32),
             pltpu.VMEM((LANES, LANES), f32),
             pltpu.VMEM((8, LANES), f32),
@@ -484,7 +478,7 @@
             dma((9,)),
             dma((7,)),
             dma((Z,)),
-            dma((N,)),
+            dma((Z,)),
             dma((N,)),
             dma((N,)),
             dma((N,)),
@@ -492,25 +486,34 @@
             dma((N,)),
             dma((Y,)),
             dma((Y,)),
-            dma((2,)),
         ],
         compiler_params=pltpu.CompilerParams(
-            collective_id=0, has_side_effects=True, vmem_limit_bytes=60 * 1024 * 1024
+            collective_id=0, has_side_effects=True, vmem_limit_bytes=36 * 1024 * 1024
         ),
         name="mixer",
     )(
-        context_input_tensor[0],
-        content_mapping_matrix,
-        address_mapping_matrix,
-        increment_mapping_matrix.T,
-        increment_speed_offset.reshape(1, 1),
-        channel_fading_exponent.reshape(1, 1),
-        extra_damping_spikes.reshape(LANES, LANES),
-        content_smoothing_coefficients.reshape(KERNEL, HEAD),
-        address_smoothing_coefficients,
-        newest_lookup_matrix[0],
-        newest_output_switch[0],
-        cluster_scaling_coefficients,
+        *map(
+            in_hbm,
+            (
+                context_input_tensor[0],
+                content_mapping_matrix,
+                address_mapping_matrix,
+                increment_mapping_matrix.T,
+            ),
+        ),
+        increment_speed_offset,
+        channel_fading_exponent,
+        *map(
+            in_hbm,
+            (
+                extra_damping_spikes.reshape(LANES, LANES),
+                content_smoothing_coefficients,
+                address_smoothing_coefficients,
+                newest_lookup_matrix[0],
+                newest_output_switch[0],
+                cluster_scaling_coefficients,
+            ),
+        ),
     )
     return (kv.reshape(1, N * SPAN, 1, LANES), read[None])
 

time: 91.9 us -> 81 us (0.88)
  the two profiles are of different devices: /device:TPU:38 before, /device:TPU:1 now
where the time goes in v2:
time: 81 us; the launch traced here: 80.9 us
  Pallas kernels  76.4 us (94%)
  local copies, waits for them, and re-layouts  2.53 us (3%)
  between operations  1.93 us (2%)
    pallas_call x1, Pallas kernels, on_device(): pl.pallas_call(kernel, out_shape=(pltpu.VMEM((N * SPAN, LANES), bf16), ja...  76.4 us
    unnamed x2, local copies, waits for them, and re-layouts  2.53 us

profile of v2, /device:TPU:1, one launch (start us, length us, event | category | flops | bytes accessed | tf_op | source)
XLA Modules:
  0.0 80.9 jit_solution(4608593148627346477)
XLA Ops:
  1.9 76.4 %mixer.1 = (bf16[16384,128]{1,0:T(8,128)(2,1)S(1)}, bf16[1,64]{1,0:T(2,128)(2,1)S(1)}) custom-call(bf16[1024,2048]{1,0:T(8,128)(2,1)} %bitcast.9, bf16[2048,1024]{1,0:T(8,128)(2,1)} %wv_hbm.1, bf16[2048,256]{1,0:T(8,128)(2,1)} %wk_hbm.1, bf16[16,2048]{1,0:T(8,128)(2,1)} %bitcast.10, f32[1]{0:T(128)S(6)} %copy.17.offset_ref, f32[1]{0:T(128)S(6)} %copy.18.fading_ref, ...), custom_call_target="tpu_custom_call" | custom-call | tf_op jit(solution)/shard_map/mixer/pallas_call | solution.py:440
  78.3 2.0 %copy.16 = bf16[1,16384,1,128]{3,1,2,0:T(8,128)(2,1)} copy(bf16[1,16384,1,128]{3,1,2,0:T(8,128)(2,1)S(1)} %bitcast.7) | data formatting | bytes 8388608
  80.3 0.5 copy.19

commit v3 on v2

--- a/solution.py
+++ b/solution.py
@@ -23,6 +23,7 @@
 MESH = pl.DeviceIdType.MESH
 CHUNK = 64
 NOTE = 48
+CUT = 288
 
 
 def mirror(place, side):
@@ -168,10 +169,25 @@
     def value_copy(slot, dest):
         return remote(sb.at[slot], rv.at[me], v_send.at[dest], v_recv.at[me], dest)
 
-    def forward_copy(zs, j):
+    def step_copy(zs, way):
         s = zs * Y + y
         return remote(
-            rk.at[s], rk.at[s], f_send.at[zs * Y + j], k_recv.at[s], z * Y + (y + j) % Y
+            rk.at[s],
+            rk.at[s],
+            f_send.at[zs * Y + (1 - way) // 2],
+            k_recv.at[s],
+            z * Y + (y + way) % Y,
+        )
+
+    def half_copy(zs, way):
+        s = zs * Y + (y - way) % Y
+        part = pl.ds(0, CUT) if way == 1 else pl.ds(CUT, HALF + NOTE - CUT)
+        return remote(
+            rk.at[s, part],
+            rk.at[s, part],
+            f_send.at[zs * Y + 2 + (1 - way) // 2],
+            k_recv.at[s] if way == 1 else n_recv.at[s],
+            z * Y + (y + way) % Y,
         )
 
     def multiply(i):
@@ -235,8 +251,8 @@
     for k in range(3):
         note_copy(steps[k]).start()
     rk[me, HALF:] = nsend[z]
-    for j in (2, 1, 3):
-        forward_copy(z, j).start()
+    for way in (1, -1):
+        step_copy(z, way).start()
 
     def tile(i, carry):
         multiply(i)
@@ -248,28 +264,35 @@
                 yd = (y + j) % Y
                 value_copy(4 * i + yd, zd * Y + yd).start()
 
-        @pl.when(i == 4)
-        def _():
-            for j in (2, 1, 3):
-                yd = (y + j) % Y
-                value_copy(16 + yd, z * Y + yd).start()
-
         return carry
 
     lax.fori_loop(1, 5, tile, 0)
     rv[me] = sb[16 + y]
 
-    for near in (1 - zr, 2 + 0 * zr, 3 + 0 * zr):
-        zs = mirror(near, side)
-        s = zs * Y + y
+    def pass_on(zs):
+        for way in (1, -1):
+            s = zs * Y + (y - way) % Y
+            remote(rk.at[0], rk.at[s], f_send.at[0], k_recv.at[s], s).wait_recv()
+            half_copy(zs, way).start()
+
+    places = [z, mirror(1 - zr, side), mirror(2 + 0 * zr, side), mirror(3 + 0 * zr, side)]
+    for i in range(1, 4):
+        s = places[i] * Y + y
         remote(sb.at[0], rk.at[s, keys], k_send.at[0], k_recv.at[s], s).wait_recv()
         remote(nsend.at[0], rk.at[s, extra], n_send.at[0], n_recv.at[s], s).wait_recv()
-        for j in (2, 1, 3):
-            forward_copy(zs, j).start()
+        for way in (1, -1):
+            step_copy(places[i], way).start()
+        pass_on(places[i - 1])
+    pass_on(places[3])
+    for j in (2, 1, 3):
+        yd = (y + j) % Y
+        value_copy(16 + yd, z * Y + yd).start()
     for zz in range(Z):
-        for j in (1, 2, 3):
-            s = zz * Y + (y + j) % Y
-            remote(rk.at[0], rk.at[s], f_send.at[0], k_recv.at[s], s).wait_recv()
+        s = zz * Y + (y + 2) % Y
+        part = pl.ds(0, CUT)
+        remote(rk.at[0, part], rk.at[s, part], f_send.at[0], k_recv.at[s], s).wait_recv()
+        part = pl.ds(CUT, HALF + NOTE - CUT)
+        remote(rk.at[0, part], rk.at[s, part], f_send.at[0], n_recv.at[s], s).wait_recv()
 
     edge_v[0] = jnp.zeros((8, LANES), jnp.float32)
     edge_k[0] = jnp.zeros((8, LANES), jnp.float32)
@@ -323,9 +346,9 @@
     def span_of(t):
         zi = t // Y
         ji = t % Y
-        zz = z * (zi == 0) + mirror(1 - zr, side) * (zi == 1)
-        zz = zz + mirror(3 - zr * 0, side) * (zi == 2) + mirror(2 + zr * 0, side) * (zi == 3)
-        j = 0 * (ji == 0) + 1 * (ji == 1) + 3 * (ji == 2) + 2 * (ji == 3)
+        place = 3 * (zi == 0) + (1 - zr) * 2 * (zi == 1) + (zi == 2) + zr * 2 * (zi == 3)
+        zz = mirror(place, side)
+        j = 2 * (ji == 0) + 3 * (ji == 1) + (ji == 2)
         return zz * Y + (y + j) % Y
 
     low_c = lo_mask(CHUNK)
@@ -333,7 +356,7 @@
     def process(t, carry):
         s = span_of(t)
 
-        @pl.when(t > 0)
+        @pl.when(s != me)
         def _():
             remote(sb.at[0], rv.at[s], v_send.at[0], v_recv.at[s], s).wait_recv()
 
@@ -412,8 +435,9 @@
         for j in range(Y):
             value_copy(4, steps[k] * Y + j).wait_send()
     for zs in range(Z):
-        for j in (1, 2, 3):
-            forward_copy(zs, j).wait_send()
+        for way in (1, -1):
+            step_copy(zs, way).wait_send()
+            half_copy(zs, way).wait_send()
 
 
 def in_hbm(a):

time: 81 us -> 76.9 us (0.949)
  the two profiles are of different devices: /device:TPU:1 before, /device:TPU:38 now
where the time goes in v3:
time: 76.9 us; the launch traced here: 76.8 us
  Pallas kernels  72.3 us (94%)
  local copies, waits for them, and re-layouts  2.53 us (3%)
  between operations  1.93 us (3%)
    pallas_call x1, Pallas kernels, on_device(): pl.pallas_call(kernel, out_shape=(pltpu.VMEM((N * SPAN, LANES), bf16), ja...  72.3 us
    unnamed x2, local copies, waits for them, and re-layouts  2.53 us

profile of v3, /device:TPU:38, one launch (start us, length us, event | category | flops | bytes accessed | tf_op | source)
XLA Modules:
  0.0 76.8 jit_solution(456623677198900177)
XLA Ops:
  1.9 72.3 %mixer.1 = (bf16[16384,128]{1,0:T(8,128)(2,1)S(1)}, bf16[1,64]{1,0:T(2,128)(2,1)S(1)}) custom-call(bf16[1024,2048]{1,0:T(8,128)(2,1)} %bitcast.9, bf16[2048,1024]{1,0:T(8,128)(2,1)} %wv_hbm.1, bf16[2048,256]{1,0:T(8,128)(2,1)} %wk_hbm.1, bf16[16,2048]{1,0:T(8,128)(2,1)} %bitcast.10, f32[1]{0:T(128)S(6)} %copy.17.offset_ref, f32[1]{0:T(128)S(6)} %copy.18.fading_ref, ...), custom_call_target="tpu_custom_call" | custom-call | tf_op jit(solution)/shard_map/mixer/pallas_call | solution.py:464
  74.2 2.0 %copy.16 = bf16[1,16384,1,128]{3,1,2,0:T(8,128)(2,1)} copy(bf16[1,16384,1,128]{3,1,2,0:T(8,128)(2,1)S(1)} %bitcast.7) | data formatting | bytes 8388608
  76.3 0.5 copy.19

commit v4 on v3

--- a/solution.py
+++ b/solution.py
@@ -118,7 +118,7 @@
         loads.append(
             pltpu.make_async_copy(wv_hbm.at[:, cols], wb.at[i + 1], in_sem.at[5 + i])
         )
-    for c in loads:
+    for c in loads[:5]:
         c.start()
     smalls = [
         pltpu.make_async_copy(a, b, small_sem.at[i])
@@ -134,8 +134,6 @@
             ]
         )
     ]
-    for c in smalls:
-        c.start()
 
     def lo_mask(rows):
         return lax.broadcasted_iota(jnp.int32, (rows, LANES), 1) < HEAD
@@ -194,19 +192,15 @@
         acc[...] = jnp.dot(xb[...], wb[i], preferred_element_type=jnp.float32)
         low = lo_mask(CHUNK)
 
-        def pack(c, carry2):
-            r0 = pl.multiple_of(c * CHUNK, CHUNK)
+        for r0 in range(0, HALF, CHUNK):
             for pair in range(2):
                 cols = slice(pair * LANES, (pair + 1) * LANES)
-                top = acc[pl.ds(r0, CHUNK), cols]
-                bot = acc[pl.ds(r0 + HALF, CHUNK), cols]
+                top = acc[r0 : r0 + CHUNK, cols]
+                bot = acc[r0 + HALF : r0 + HALF + CHUNK, cols]
                 even = jnp.where(low, top, swap(bot))
                 odd = jnp.where(low, swap(top), bot)
-                sb[4 * i + 2 * pair, pl.ds(r0, CHUNK)] = even.astype(jnp.bfloat16)
-                sb[4 * i + 2 * pair + 1, pl.ds(r0, CHUNK)] = odd.astype(jnp.bfloat16)
-            return carry2
-
-        lax.fori_loop(0, HALF // CHUNK, pack, 0)
+                sb[4 * i + 2 * pair, r0 : r0 + CHUNK] = even.astype(jnp.bfloat16)
+                sb[4 * i + 2 * pair + 1, r0 : r0 + CHUNK] = odd.astype(jnp.bfloat16)
 
     low8 = lo_mask(8)
 
@@ -222,8 +216,10 @@
 
     notes[...] = jnp.zeros_like(notes)
 
-    for i in range(5):
-        loads[i].wait()
+    for c in loads[:5]:
+        c.wait()
+    for c in loads[5:] + smalls:
+        c.start()
     multiply(0)
     pl.semaphore_wait(barrier, N - 1)
     for k in range(3):

time: 76.9 us -> 76.2 us (level)
  no operation moved by 1% of the time
where the time goes in v4:
time: 76.2 us; the launch traced here: 76.1 us
  Pallas kernels  71.7 us (94%)
  local copies, waits for them, and re-layouts  2.53 us (3%)
  between operations  1.93 us (3%)
    pallas_call x1, Pallas kernels, on_device(): pl.pallas_call(kernel, out_shape=(pltpu.VMEM((N * SPAN, LANES), bf16), ja...  71.7 us
    unnamed x2, local copies, waits for them, and re-layouts  2.53 us

profile of v4, /device:TPU:38, one launch (start us, length us, event | category | flops | bytes accessed | tf_op | source)
XLA Modules:
  0.0 76.1 jit_solution(6323609361161314336)
XLA Ops:
  1.9 71.7 %mixer.1 = (bf16[16384,128]{1,0:T(8,128)(2,1)S(1)}, bf16[1,64]{1,0:T(2,128)(2,1)S(1)}) custom-call(bf16[1024,2048]{1,0:T(8,128)(2,1)} %bitcast.9, bf16[2048,1024]{1,0:T(8,128)(2,1)} %wv_hbm.1, bf16[2048,256]{1,0:T(8,128)(2,1)} %wk_hbm.1, bf16[16,2048]{1,0:T(8,128)(2,1)} %bitcast.10, f32[1]{0:T(128)S(6)} %copy.17.offset_ref, f32[1]{0:T(128)S(6)} %copy.18.fading_ref, ...), custom_call_target="tpu_custom_call" | custom-call | tf_op jit(solution)/shard_map/mixer/pallas_call | solution.py:460
  73.6 2.0 %copy.16 = bf16[1,16384,1,128]{3,1,2,0:T(8,128)(2,1)} copy(bf16[1,16384,1,128]{3,1,2,0:T(8,128)(2,1)S(1)} %bitcast.7) | data formatting | bytes 8388608
  75.6 0.5 copy.19

commit v5 on v4

--- a/solution.py
+++ b/solution.py
@@ -24,6 +24,7 @@
 CHUNK = 64
 NOTE = 48
 CUT = 288
+PART = HALF // 2
 
 
 def mirror(place, side):
@@ -31,7 +32,8 @@
 
 
 def silu(v):
-    return v / (1.0 + jnp.exp(-v))
+    half = 0.5 * v
+    return half + half * jnp.tanh(half)
 
 
 def kernel(
@@ -89,6 +91,8 @@
     v_recv,
     g_send,
     g_recv,
+    h_recv,
+    ready,
 ):
     me = lax.axis_index("sp")
     z = me // Y
@@ -103,16 +107,16 @@
     steps = [mirror(first, side), mirror(second, side), mirror(third, side), z]
 
     barrier = pltpu.get_barrier_semaphore()
-    for i in range(1, N):
-        pl.semaphore_signal(
-            barrier, inc=1, device_id={"sp": (me + i) % N}, device_id_type=MESH
-        )
+    column = [((z + i) % Z) * Y + y for i in range(1, Z)]
+    row = [z * Y + (y + i) % Y for i in range(1, Y)]
+    for peer in column + row:
+        pl.semaphore_signal(barrier, inc=1, device_id={"sp": peer}, device_id_type=MESH)
 
     loads = []
-    for i in range(4):
-        rows = pl.ds(i * 256, 256)
+    for i in (0, 2, 1, 3):
+        rows = pl.ds(i * PART, PART)
         loads.append(pltpu.make_async_copy(x_hbm.at[rows], xb.at[rows], in_sem.at[i]))
-    loads.append(pltpu.make_async_copy(wk_hbm, wb.at[0], in_sem.at[4]))
+    loads.insert(0, pltpu.make_async_copy(wk_hbm, wb.at[0], in_sem.at[4]))
     for i in range(4):
         cols = pl.ds(pl.multiple_of(steps[i] * 256, 256), 256)
         loads.append(
@@ -151,12 +155,16 @@
             device_id_type=MESH,
         )
 
-    keys = pl.ds(0, HALF)
+    keys = (pl.ds(0, PART), pl.ds(PART, PART))
     extra = pl.ds(HALF, NOTE)
 
-    def key_copy(zd):
+    def key_copy(zd, part):
         return remote(
-            sb.at[zd], rk.at[me, keys], k_send.at[zd], k_recv.at[me], zd * Y + y
+            sb.at[zd, keys[part]],
+            rk.at[me, keys[part]],
+            k_send.at[part * Z + zd],
+            (k_recv, h_recv)[part].at[me],
+            zd * Y + y,
         )
 
     def note_copy(zd):
@@ -190,9 +198,11 @@
 
     def multiply(i):
         acc[...] = jnp.dot(xb[...], wb[i], preferred_element_type=jnp.float32)
+        pack(i, 0, HALF)
+
+    def pack(i, start, stop):
         low = lo_mask(CHUNK)
-
-        for r0 in range(0, HALF, CHUNK):
+        for r0 in range(start, stop, CHUNK):
             for pair in range(2):
                 cols = slice(pair * LANES, (pair + 1) * LANES)
                 top = acc[r0 : r0 + CHUNK, cols]
@@ -216,14 +226,25 @@
 
     notes[...] = jnp.zeros_like(notes)
 
-    for c in loads[:5]:
-        c.wait()
-    for c in loads[5:] + smalls:
-        c.start()
-    multiply(0)
-    pl.semaphore_wait(barrier, N - 1)
-    for k in range(3):
-        key_copy(steps[k]).start()
+    for part in range(2):
+        for c in loads[2 * part + (part > 0) : 2 * part + 3]:
+            c.wait()
+        if part == 1:
+            for c in loads[5:] + smalls:
+                c.start()
+        for r0 in (PART * part, HALF + PART * part):
+            acc[r0 : r0 + PART] = jnp.dot(
+                xb[r0 : r0 + PART], wb[0], preferred_element_type=jnp.float32
+            )
+        pack(0, PART * part, PART * part + PART)
+        if part == 0:
+            pl.semaphore_wait(barrier, Z + Y - 2)
+            for peer in column:
+                pl.semaphore_signal(
+                    ready.at[z], inc=1, device_id={"sp": peer}, device_id_type=MESH
+                )
+        for k in range(3):
+            key_copy(steps[k], part).start()
     rk[me, 0:HALF] = sb[z]
 
     for g, e in enumerate(edge_rows(acc[0:8], acc[SPAN - 8 : SPAN])):
@@ -256,6 +277,7 @@
 
         @pl.when(i < 4)
         def _():
+            pl.semaphore_wait(ready.at[zd], 1)
             for j in (2, 1, 3, 0):
                 yd = (y + j) % Y
                 value_copy(4 * i + yd, zd * Y + yd).start()
@@ -274,7 +296,8 @@
     places = [z, mirror(1 - zr, side), mirror(2 + 0 * zr, side), mirror(3 + 0 * zr, side)]
     for i in range(1, 4):
         s = places[i] * Y + y
-        remote(sb.at[0], rk.at[s, keys], k_send.at[0], k_recv.at[s], s).wait_recv()
+        for part, sem in ((keys[0], k_recv), (keys[1], h_recv)):
+            remote(sb.at[0, part], rk.at[s, part], k_send.at[0], sem.at[s], s).wait_recv()
         remote(nsend.at[0], rk.at[s, extra], n_send.at[0], n_recv.at[s], s).wait_recv()
         for way in (1, -1):
             step_copy(places[i], way).start()
@@ -349,53 +372,65 @@
 
     low_c = lo_mask(CHUNK)
 
-    def process(t, carry):
+    def extend(block, edge, s, ext):
+        block = block.astype(jnp.float32)
+        ext[8 : 8 + HALF] = block
+        ext[0:8] = jnp.where(low8, edge[s], swap(block[HALF - 8 : HALF]))
+        ext[8 + HALF : 16 + HALF] = jnp.where(low8, swap(block[0:8]), edge[s + 2])
+
+    def convolved(ext, tap, r0):
+        total = tap[0:1] * ext[r0 + 6 : r0 + 6 + CHUNK]
+        for k in range(1, KERNEL):
+            total = total + tap[k : k + 1] * ext[r0 + 6 + k : r0 + 6 + k + CHUNK]
+        return silu(total)
+
+    def convolve_keys(s, carry):
+        extend(rk[s, 0:HALF], edge_k, s, extk)
+        for r0 in range(0, HALF, CHUNK):
+            kc[s, r0 : r0 + CHUNK] = convolved(extk, tapk, r0).astype(jnp.bfloat16)
+        return carry
+
+    lax.fori_loop(0, N, convolve_keys, 0)
+
+    def write_rows(s, r0, v):
+        base = pl.multiple_of(s * SPAN, SPAN) + r0
+        k = kc[s, r0 : r0 + CHUNK].astype(jnp.float32)
+        kv_out[pl.ds(base, CHUNK)] = jnp.where(low_c, v, swap(k)).astype(jnp.bfloat16)
+        kv_out[pl.ds(base + HALF, CHUNK)] = jnp.where(low_c, swap(v), k).astype(jnp.bfloat16)
+
+    def process(t, write):
         s = span_of(t)
 
         @pl.when(s != me)
         def _():
             remote(sb.at[0], rv.at[s], v_send.at[0], v_recv.at[s], s).wait_recv()
 
-        for buf, ext, edge in ((rv, extv, edge_v), (rk, extk, edge_k)):
-            block = buf[s, 0:HALF].astype(jnp.float32)
-            ext[8 : 8 + HALF] = block
-            head = swap(block[0:8])
-            tail = swap(block[HALF - 8 : HALF])
-            ext[0:8] = jnp.where(low8, edge[s], tail)
-            ext[8 + HALF : 16 + HALF] = jnp.where(low8, head, edge[s + 2])
-
-        base = pl.multiple_of(s * SPAN, SPAN)
+        extend(rv[s], edge_v, s, extv)
         w8 = weights[pl.ds(pl.multiple_of(8 * s, 8), 8)]
         wcols = jnp.transpose(jnp.concatenate([w8] * 16, axis=0))
-        tv = [tapv[k : k + 1, :] for k in range(KERNEL)]
-        tk = [tapk[k : k + 1, :] for k in range(KERNEL)]
-        for c in range(HALF // CHUNK):
-            r0 = c * CHUNK
-            v = tv[0] * extv[r0 + 6 : r0 + 6 + CHUNK]
-            kk = tk[0] * extk[r0 + 6 : r0 + 6 + CHUNK]
-            for k in range(1, KERNEL):
-                v = v + tv[k] * extv[r0 + 6 + k : r0 + 6 + k + CHUNK]
-                kk = kk + tk[k] * extk[r0 + 6 + k : r0 + 6 + k + CHUNK]
-            v = silu(v)
-            kk = silu(kk)
+        for r0 in range(0, HALF, CHUNK):
+            v = convolved(extv, tapv, r0)
             b = r0 // LANES
             p0 = r0 % LANES
             wl = wcols[p0 : p0 + CHUNK, b : b + 1]
             wh = wcols[p0 : p0 + CHUNK, b + 4 : b + 5]
+            vb = v.astype(jnp.bfloat16)
             w = jnp.where(low_c, wl, wh)
-            vb = v.astype(jnp.bfloat16)
             vw[r0 : r0 + CHUNK] = (vb.astype(jnp.float32) * w).astype(jnp.bfloat16)
-            kc[r0 : r0 + CHUNK] = kk.astype(jnp.bfloat16)
-            kv_out[pl.ds(base + r0, CHUNK)] = jnp.where(low_c, v, swap(kk)).astype(jnp.bfloat16)
-            kv_out[pl.ds(base + HALF + r0, CHUNK)] = jnp.where(low_c, swap(v), kk).astype(
-                jnp.bfloat16
-            )
+            if write:
+                write_rows(s, r0, v)
+            else:
+                rv[s, r0 : r0 + CHUNK] = vb
         states[...] += lax.dot_general(
-            kc[...], vw[...], (((0,), (0,)), ((), ())), preferred_element_type=jnp.float32
-        )
+            kc[s], vw[...], (((0,), (0,)), ((), ())), preferred_element_type=jnp.float32
+        )
+
+    def process_step(t, carry):
+        process(t, True)
         return carry
 
-    lax.fori_loop(0, N, process, 0)
+    lax.fori_loop(0, N - 1, process_step, 0)
+    process(N - 1, False)
 
     read = jnp.sum(states[...] * qmat[...], axis=0, keepdims=True)
     read = read + swap(read)
@@ -413,6 +448,9 @@
     for j in (2, 1, 3):
         square_copy(j).start()
     grecv[y] = gsend[...]
+    last = span_of(N - 1)
+    for r0 in range(0, HALF, CHUNK):
+        write_rows(last, r0, rv[last, r0 : r0 + CHUNK].astype(jnp.float32))
     for j in (1, 2, 3):
         yy = (y + j) % Y
         remote(gsend, grecv.at[yy], g_send.at[0], g_recv.at[yy], me).wait_recv()
@@ -426,7 +464,8 @@
         square_copy(j).wait_send()
         value_copy(16, z * Y + (y + j) % Y).wait_send()
     for k in range(3):
-        key_copy(steps[k]).wait_send()
+        for part in range(2):
+            key_copy(steps[k], part).wait_send()
         note_copy(steps[k]).wait_send()
         for j in range(Y):
             value_copy(4, steps[k] * Y + j).wait_send()
@@ -490,14 +529,14 @@
             pltpu.VMEM((8, LANES), f32),
             pltpu.VMEM((8, LANES), f32),
             pltpu.VMEM((HALF, LANES), bf16),
-            pltpu.VMEM((HALF, LANES), bf16),
+            pltpu.VMEM((N, HALF, LANES), bf16),
             pltpu.VMEM((LANES, LANES), f32),
             pltpu.VMEM((LANES, LANES), f32),
             pltpu.VMEM((8, LANES), f32),
             pltpu.VMEM((Y, 8, LANES), f32),
             dma((9,)),
             dma((7,)),
-            dma((Z,)),
+            dma((2 * Z,)),
             dma((Z,)),
             dma((N,)),
             dma((N,)),
@@ -506,6 +545,8 @@
             dma((N,)),
             dma((Y,)),
             dma((Y,)),
+            dma((N,)),
+            pltpu.SemaphoreType.REGULAR((Z,)),
         ],
         compiler_params=pltpu.CompilerParams(
             collective_id=0, has_side_effects=True, vmem_limit_bytes=36 * 1024 * 1024

time: 76.2 us -> 75.3 us (0.988); the launches traced: 76.1 us -> 73.9 us
  Pallas kernels: 71.7 us -> 69.5 us
    pallas_call x1, Pallas kernels: 71.7 us -> 69.5 us  [on_device(): pl.pallas_call(kernel, out_shape=(pltpu.VMEM((N * SPAN, LANES), bf16), ja...]
where the time goes in v5:
time: 75.3 us; the launch traced here: 73.9 us
  Pallas kernels  69.5 us (92%)
  local copies, waits for them, and re-layouts  2.53 us (3%)
  between operations  1.93 us (3%)
    pallas_call x1, Pallas kernels, on_device(): pl.pallas_call(kernel, out_shape=(pltpu.VMEM((N * SPAN, LANES), bf16), ja...  69.5 us
    unnamed x2, local copies, waits for them, and re-layouts  2.53 us

profile of v5, /device:TPU:38, one launch (start us, length us, event | category | flops | bytes accessed | tf_op | source)
XLA Modules:
  0.0 73.9 jit_solution(11019896497505019606)
XLA Ops:
  1.9 69.5 %mixer.1 = (bf16[16384,128]{1,0:T(8,128)(2,1)S(1)}, bf16[1,64]{1,0:T(2,128)(2,1)S(1)}) custom-call(bf16[1024,2048]{1,0:T(8,128)(2,1)} %bitcast.9, bf16[2048,1024]{1,0:T(8,128)(2,1)} %wv_hbm.1, bf16[2048,256]{1,0:T(8,128)(2,1)} %wk_hbm.1, bf16[16,2048]{1,0:T(8,128)(2,1)} %bitcast.10, f32[1]{0:T(128)S(6)} %copy.17.offset_ref, f32[1]{0:T(128)S(6)} %copy.18.fading_ref, ...), custom_call_target="tpu_custom_call" | custom-call | tf_op jit(solution)/shard_map/mixer/pallas_call | solution.py:499
  71.4 2.0 %copy.16 = bf16[1,16384,1,128]{3,1,2,0:T(8,128)(2,1)} copy(bf16[1,16384,1,128]{3,1,2,0:T(8,128)(2,1)S(1)} %bitcast.7) | data formatting | bytes 8388608
  73.4 0.5 copy.19

commit v6 on v5

--- a/solution.py
+++ b/solution.py
@@ -70,6 +70,8 @@
     edge_k,
     rates,
     weights,
+    chooser,
+    spread,
     extv,
     extk,
     tapv,
@@ -332,7 +334,7 @@
         edge_k[s + 1] = jnp.where(even, got[40:41], got[41:42])
         return carry
 
-    lax.fori_loop(0, N, unpack, 0)
+    lax.fori_loop(0, N, unpack, 0, unroll=4)
     speed = rates[...] + offset_ref[0]
     speed = jnp.maximum(speed, 0.0) + jnp.log1p(jnp.exp(-jnp.abs(speed)))
     log_step = -jnp.exp(jnp.full((1, LANES), fading_ref[0], jnp.float32)) * speed + spikes[...]
@@ -347,7 +349,17 @@
         later_row, log_step, precision=lax.Precision.HIGHEST, preferred_element_type=jnp.float32
     )
     suffix = inner + jnp.sum(outer, axis=1, keepdims=True)
-    weights[...] = speed * jnp.exp(suffix)
+    weight = speed * jnp.exp(suffix)
+    for part in range(3):
+        piece = weight.astype(jnp.bfloat16).astype(jnp.float32)
+        weight = weight - piece
+        for s in range(N):
+            weights[24 * s + 8 * part : 24 * s + 8 * part + 8] = piece[8 * s : 8 * s + 8]
+    shape = (24, HALF)
+    wanted = lax.broadcasted_iota(jnp.int32, shape, 1)
+    wanted = wanted // LANES + Y * (wanted % LANES >= HEAD)
+    pick = lax.broadcasted_iota(jnp.int32, shape, 0) % 8 == wanted
+    chooser[...] = pick.astype(jnp.float32).astype(jnp.bfloat16)
 
     for k in range(KERNEL):
         row = vtaps_s[k]
@@ -406,21 +418,20 @@
             remote(sb.at[0], rv.at[s], v_send.at[0], v_recv.at[s], s).wait_recv()
 
         extend(rv[s], edge_v, s, extv)
-        w8 = weights[pl.ds(pl.multiple_of(8 * s, 8), 8)]
-        wcols = jnp.transpose(jnp.concatenate([w8] * 16, axis=0))
+        parts = weights[pl.ds(pl.multiple_of(24 * s, 8), 24)].astype(jnp.bfloat16)
+        spread[...] = lax.dot_general(
+            parts, chooser[...], (((0,), (0,)), ((), ())), preferred_element_type=jnp.float32
+        )
         for r0 in range(0, HALF, CHUNK):
             v = convolved(extv, tapv, r0)
             b = r0 // LANES
             p0 = r0 % LANES
-            wl = wcols[p0 : p0 + CHUNK, b : b + 1]
-            wh = wcols[p0 : p0 + CHUNK, b + 4 : b + 5]
-            vb = v.astype(jnp.bfloat16)
-            w = jnp.where(low_c, wl, wh)
-            vw[r0 : r0 + CHUNK] = (vb.astype(jnp.float32) * w).astype(jnp.bfloat16)
+            w = spread[p0 : p0 + CHUNK, b * LANES : (b + 1) * LANES]
+            vw[r0 : r0 + CHUNK] = (v * w).astype(jnp.bfloat16)
             if write:
                 write_rows(s, r0, v)
             else:
-                rv[s, r0 : r0 + CHUNK] = vb
+                rv[s, r0 : r0 + CHUNK] = v.astype(jnp.bfloat16)
         states[...] += lax.dot_general(
             kc[s], vw[...], (((0,), (0,)), ((), ())), preferred_element_type=jnp.float32
         )
@@ -523,7 +534,9 @@
             pltpu.VMEM((N + 2, 8, LANES), f32),
             pltpu.VMEM((N + 2, 8, LANES), f32),
             pltpu.VMEM((LANES, LANES), f32),
-            pltpu.VMEM((LANES, LANES), f32),
+            pltpu.VMEM((24 * N, LANES), f32),
+            pltpu.VMEM((24, HALF), bf16),
+            pltpu.VMEM((LANES, HALF), f32),
             pltpu.VMEM((HALF + 16, LANES), f32),
             pltpu.VMEM((HALF + 16, LANES), f32),
             pltpu.VMEM((8, LANES), f32),

time: 75.3 us -> 73.9 us (0.981); the launches traced: 73.9 us -> 73.8 us
  no operation moved by 1% of the time
where the time goes in v6:
time: 73.9 us; the launch traced here: 73.8 us
  Pallas kernels  69.3 us (94%)
  local copies, waits for them, and re-layouts  2.53 us (3%)
  between operations  1.93 us (3%)
    pallas_call x1, Pallas kernels, on_device(): pl.pallas_call(kernel, out_shape=(pltpu.VMEM((N * SPAN, LANES), bf16), ja...  69.3 us
    unnamed x2, local copies, waits for them, and re-layouts  2.53 us

profile of v6, /device:TPU:38, one launch (start us, length us, event | category | flops | bytes accessed | tf_op | source)
XLA Modules:
  0.0 73.8 jit_solution(4658579862712117871)
XLA Ops:
  1.9 69.3 %mixer.1 = (bf16[16384,128]{1,0:T(8,128)(2,1)S(1)}, bf16[1,64]{1,0:T(2,128)(2,1)S(1)}) custom-call(bf16[1024,2048]{1,0:T(8,128)(2,1)} %bitcast.9, bf16[2048,1024]{1,0:T(8,128)(2,1)} %wv_hbm.1, bf16[2048,256]{1,0:T(8,128)(2,1)} %wk_hbm.1, bf16[16,2048]{1,0:T(8,128)(2,1)} %bitcast.10, f32[1]{0:T(128)S(6)} %copy.17.offset_ref, f32[1]{0:T(128)S(6)} %copy.18.fading_ref, ...), custom_call_target="tpu_custom_call" | custom-call | tf_op jit(solution)/shard_map/mixer/pallas_call | solution.py:510
  71.3 2.0 %copy.16 = bf16[1,16384,1,128]{3,1,2,0:T(8,128)(2,1)} copy(bf16[1,16384,1,128]{3,1,2,0:T(8,128)(2,1)S(1)} %bitcast.7) | data formatting | bytes 8388608
  73.3 0.5 copy.19

commit v7 on v6

--- a/solution.py
+++ b/solution.py
@@ -25,6 +25,7 @@
 NOTE = 48
 CUT = 288
 PART = HALF // 2
+PIECES = 4
 
 
 def mirror(place, side):
@@ -484,6 +485,18 @@
         for way in (1, -1):
             step_copy(zs, way).wait_send()
             half_copy(zs, way).wait_send()
+
+
+def hand_out(kv_in, read_in, kv_out, read_out, sem):
+    size = N * SPAN // PIECES
+    copies = [pltpu.make_async_copy(read_in, read_out, sem.at[PIECES])]
+    for i in range(PIECES):
+        rows = pl.ds(i * size, size)
+        copies.append(pltpu.make_async_copy(kv_in.at[rows], kv_out.at[rows], sem.at[i]))
+    for c in copies:
+        c.start()
+    for c in copies:
+        c.wait()
 
 
 def in_hbm(a):
@@ -589,6 +602,19 @@
             ),
         ),
     )
+    on_chip = pl.BlockSpec(memory_space=pltpu.VMEM)
+    kv, read = pl.pallas_call(
+        hand_out,
+        out_shape=(
+            jax.ShapeDtypeStruct((N * SPAN, LANES), bf16),
+            jax.ShapeDtypeStruct((1, HEAD), bf16),
+        ),
+        in_specs=[on_chip, on_chip],
+        out_specs=(anywhere, anywhere),
+        scratch_shapes=[dma((PIECES + 1,))],
+        compiler_params=pltpu.CompilerParams(vmem_limit_bytes=8 * 1024 * 1024),
+        name="hand_out",
+    )(*(pltpu.with_memory_space_constraint(a, pltpu.VMEM) for a in (kv, read)))
     return (kv.reshape(1, N * SPAN, 1, LANES), read[None])
 
 

time: 73.9 us -> 73.4 us (level)
  local copies, waits for them, and re-layouts: 2.53 us -> 0 us
  Pallas kernels: 69.3 us -> 71.4 us
    unnamed x2 -> x0, local copies, waits for them, and re-layouts: 2.53 us -> none
    pallas_call x0 -> x1, Pallas kernels: none -> 2.05 us  [on_device(): pl.pallas_call(hand_out, out_shape=(jax.ShapeDtypeStruct((N * SPAN, LANES...]
where the time goes in v7:
time: 73.4 us; the launch traced here: 73.3 us
  Pallas kernels  71.4 us (97%)
  between operations  1.93 us (3%)
    pallas_call x1, Pallas kernels, on_device(): pl.pallas_call(kernel, out_shape=(pltpu.VMEM((N * SPAN, LANES), bf16), ja...  69.3 us
    pallas_call x1, Pallas kernels, on_device(): pl.pallas_call(hand_out, out_shape=(jax.ShapeDtypeStruct((N * SPAN, LANES...  2.05 us

profile of v7, /device:TPU:38, one launch (start us, length us, event | category | flops | bytes accessed | tf_op | source)
XLA Modules:
  0.0 73.3 jit_solution(15392968840871404667)
XLA Ops:
  1.9 69.3 %mixer.1 = (bf16[16384,128]{1,0:T(8,128)(2,1)S(1)}, bf16[1,64]{1,0:T(2,128)(2,1)S(1)}) custom-call(bf16[1024,2048]{1,0:T(8,128)(2,1)} %bitcast.7, bf16[2048,1024]{1,0:T(8,128)(2,1)} %wv_hbm.1, bf16[2048,256]{1,0:T(8,128)(2,1)} %wk_hbm.1, bf16[16,2048]{1,0:T(8,128)(2,1)} %bitcast.8, f32[1]{0:T(128)S(6)} %copy.14.offset_ref, f32[1]{0:T(128)S(6)} %copy.15.fading_ref, ...), custom_call_target="tpu_custom_call" | custom-call | tf_op jit(solution)/shard_map/mixer/pallas_call | solution.py:523
  71.3 2.1 %hand_out.1 = (bf16[16384,128]{1,0:T(8,128)(2,1)}, bf16[1,64]{1,0:T(2,128)(2,1)}) custom-call(bf16[16384,128]{1,0:T(8,128)(2,1)S(1)} %get-tuple-element.6.kv_in, bf16[1,64]{1,0:T(2,128)(2,1)S(1)} %get-tuple-element.7.read_in), custom_call_target="tpu_custom_call" | custom-call | tf_op jit(solution)/shard_map/hand_out/pallas_call | solution.py:606
